TPU v7x, 32 devices: a whole 2x2x4 slice. The times are simulated.
32 devices in a mesh: ep: 8 (over z, x), tp: 4 (over y, core).
Axes of the slice: x: 2, y: 2, z: 4, core: 2. Of those that a mesh axis runs over, the one named last changes fastest.
Arguments:
- queries: bfloat16 [8192, 2048], P('ep', 'tp'), may hold values from -128 to 128
- key_heads: bfloat16 [8192, 1024], P('ep', 'tp'), may hold values from -6 to 6
- value_heads: bfloat16 [8192, 1024], P('ep', 'tp'), may hold values from -6 to 6
- sink_logits: float32 [32], P('tp'), may hold values from 1 to 5
- mix_weight: bfloat16 [2048, 2048], replicated, may hold values from -1 to 1
- expert_input: bfloat16 [4096, 2048], P(('ep', 'tp')), may hold values from -6 to 6
- norm_gain: float32 [2048], replicated, may hold values from 0.1 to 1.9
- routes: int32 [4096, 4], P(('ep', 'tp')), may hold values from 0 to 31, all different within a row; in each aligned block of 128 rows (0 to 127, 128 to 255, ...) at most 32 rows name the same one
- route_weights: float32 [4096, 4], P(('ep', 'tp')), may hold values from 0.1 to 1
- gate_weight: bfloat16 [32, 2048, 1024], P(('ep', 'tp')), may hold values from -0.375 to 0.375
- up_weight: bfloat16 [32, 2048, 1024], P(('ep', 'tp')), may hold values from -0.375 to 0.375
- down_weight: bfloat16 [32, 1024, 2048], P(('ep', 'tp')), may hold values from -0.046875 to 0.046875
Outputs:
- mixer_out: bfloat16 [8192, 2048], P(('ep', 'tp'))
- experts_out: bfloat16 [4096, 2048], P(('ep', 'tp'))
Inputs may be any that keep to these rules, and one draw needn't show every extreme that they name: `routes`: each row names 4 different experts; within the 128 rows of one device no expert is named more than 32 times, and in some devices' rows some expert is named exactly 32 times.
All inputs are finite; a program needn't handle non-finite values.
Results may differ from a plain program's by a relative error of at most 0.012.
The roundings to bfloat16 on the way count: a program that leaves them out, or rounds other values in their place, can miss the bound.
Values may be sent and summed in bfloat16 or wider, within the bound.
A program may use at most 128 MiB of HBM per device.

v0:
```python
import functools
import math

import jax
import jax.numpy as jnp
from jax import lax
from jax.experimental import pallas as pl
from jax.experimental.pallas import tpu as pltpu
from jax.sharding import Mesh
from jax.sharding import PartitionSpec as P

HEAD_DIM = 64
WINDOW = 128
GRID_W = 64
ROPE_BASE = 10000.0
CLAMP_LIMIT = 7.0
GATE_SLOPE = 1.702
NORM_EPS = 1e-05

F32 = jnp.float32
BF16 = jnp.bfloat16


def angle_tables(first, rows):
    half = HEAD_DIM // 2
    quarter = HEAD_DIM // 4
    lane = jnp.arange(2 * HEAD_DIM, dtype=jnp.int32) % HEAD_DIM
    freqs = ROPE_BASE ** (-jnp.arange(0, half, 2, dtype=F32) / half)
    lane_freq = jnp.tile(freqs, 2 * HEAD_DIM // quarter)
    by_row = (first // GRID_W + jnp.arange(rows // GRID_W, dtype=jnp.int32)).astype(F32)
    by_col = (jnp.arange(WINDOW, dtype=jnp.int32) % GRID_W).astype(F32)
    angle = jnp.concatenate([by_row, by_col])[:, None] * lane_freq[None, :]
    sign = jnp.where(lane % half < quarter, -1.0, 1.0).astype(F32)
    return jnp.cos(angle), jnp.sin(angle) * sign[None, :]


def turn(cells, cosines, sines):
    quarter = HEAD_DIM // 4
    width = cells.shape[1]
    lane = lax.broadcasted_iota(jnp.int32, cells.shape, 1)
    ahead = pltpu.roll(cells, width - quarter, 1)
    behind = pltpu.roll(cells, quarter, 1)
    partner = jnp.where(lane % (2 * quarter) < quarter, ahead, behind)
    return cells * cosines + partner * sines

MESH = pl.DeviceIdType.MESH


def kernel(
    sizes,
    sink,
    route_ref,
    x_ref,
    gain_ref,
    q_ref,
    k_ref,
    v_ref,
    cos_ref,
    sin_ref,
    wg_hbm,
    wu_hbm,
    wd_hbm,
    mix_hbm,
    mixer_ref,
    expert_ref,
    k_scr,
    v_scr,
    halo,
    att,
    att_in,
    routing,
    normed,
    outgoing,
    arrived,
    produced,
    returned,
    shares,
    partial,
    home,
    wg,
    wu,
    wd,
    mix,
    act,
    z_send,
    z_recv,
    rt_send,
    rt_recv,
    out_send,
    out_recv,
    back_send,
    back_recv,
    home_send,
    home_recv,
    att_send,
    att_recv,
    halo_send,
    halo_recv,
    load_sem,
):
    n_z, n_x, n_tp, top_count, capacity = sizes
    n_ep = n_z * n_x
    plane = n_x * n_tp
    slots = plane * capacity
    z, x, t = lax.axis_index("zz"), lax.axis_index("xx"), lax.axis_index("tp")
    me = x * n_tp + t
    ep = z * n_x + x
    rows_here, width_q = q_ref.shape
    tok, width = x_ref.shape
    length = rows_here * n_ep
    kv_local = k_scr.shape[0]
    bq = WINDOW
    span = bq + 2 * WINDOW
    blocks = rows_here // bq
    chunk = rows_here // n_tp

    def z_dev(b):
        return (b, x, t)

    def plane_dev(p):
        return (z, lax.div(p, n_tp), lax.rem(p, n_tp))

    def ep_dev(e):
        return (lax.div(e, n_x), lax.rem(e, n_x), t)

    after, before = lax.rem(ep + 1, n_ep), lax.rem(ep + n_ep - 1, n_ep)

    loads = [
        pltpu.make_async_copy(wg_hbm.at[0], wg, load_sem.at[0]),
        pltpu.make_async_copy(wu_hbm.at[0], wu, load_sem.at[1]),
        pltpu.make_async_copy(wd_hbm.at[0], wd, load_sem.at[2]),
        pltpu.make_async_copy(mix_hbm, mix, load_sem.at[3]),
    ]
    for load in loads:
        load.start()

    barrier = pltpu.get_barrier_semaphore()

    def greet_z(o, _):
        pl.semaphore_signal(barrier, inc=1, device_id=z_dev(lax.rem(z + o, n_z)), device_id_type=MESH)
        return 0

    def greet_plane(p, _):
        pl.semaphore_signal(
            barrier, inc=1, device_id=plane_dev(lax.rem(me + p, plane)), device_id_type=MESH
        )
        return 0

    lax.fori_loop(1, n_z, greet_z, 0)
    lax.fori_loop(1, plane, greet_plane, 0)
    for e in (after, before):
        pl.semaphore_signal(barrier, inc=1, device_id=ep_dev(e), device_id_type=MESH)

    for part in range(tok // 32):
        rows = slice(part * 32, part * 32 + 32)
        values = x_ref[rows, :].astype(F32)
        center = jnp.mean(values, axis=1, keepdims=True)
        spread = jnp.mean(jnp.square(values - center), axis=1, keepdims=True)
        normed[z, rows, :] = (
            (values - center) * lax.rsqrt(spread + NORM_EPS) * gain_ref[...]
        ).astype(BF16)
    routing[z] = route_ref[...]
    pl.semaphore_wait(barrier, n_z - 1 + plane - 1 + 2)

    def rt_copy(o):
        return pltpu.make_async_remote_copy(
            src_ref=routing.at[z],
            dst_ref=routing.at[z],
            send_sem=rt_send.at[o],
            recv_sem=rt_recv.at[z],
            device_id=z_dev(lax.rem(z + o, n_z)),
            device_id_type=MESH,
        )

    def z_copy(o):
        return pltpu.make_async_remote_copy(
            src_ref=normed.at[z],
            dst_ref=normed.at[z],
            send_sem=z_send.at[o],
            recv_sem=z_recv.at[z],
            device_id=z_dev(lax.rem(z + o, n_z)),
            device_id_type=MESH,
        )

    def halo_copy(source, which, start, target):
        return pltpu.make_async_remote_copy(
            src_ref=source.at[pl.ds(start, WINDOW)],
            dst_ref=halo.at[which],
            send_sem=halo_send.at[which],
            recv_sem=halo_recv.at[which],
            device_id=ep_dev(target),
            device_id_type=MESH,
        )

    halos = [
        halo_copy(k_ref, 0, rows_here - WINDOW, after),
        halo_copy(v_ref, 1, rows_here - WINDOW, after),
        halo_copy(k_ref, 2, 0, before),
        halo_copy(v_ref, 3, 0, before),
    ]
    for o in range(1, n_z):
        rt_copy(o).start()
    for copy in halos:
        copy.start()
    for o in range(1, n_z):
        z_copy(o).start()

    def await_bytes(ref, sem):
        pltpu.make_async_copy(ref, ref, sem).wait()

    def source_of(o):
        return lax.rem(z + n_z - o, n_z)

    slot_row = lax.broadcasted_iota(jnp.int32, (slots, tok), 0)
    lane_expert = (z * plane + lax.div(slot_row, capacity)).astype(F32)
    place_in = lax.rem(slot_row, capacity).astype(F32)
    upper = (
        lax.broadcasted_iota(jnp.int32, (tok, tok), 0) < lax.broadcasted_iota(jnp.int32, (tok, tok), 1)
    ).astype(F32).astype(BF16)

    def dispatch(o):
        b = source_of(o)
        if o > 0:
            await_bytes(routing.at[b], rt_recv.at[b])
            await_bytes(normed.at[b], z_recv.at[b])
        route = routing[b]
        member = jnp.zeros((slots, tok), F32)
        share = jnp.zeros((slots, tok), F32)
        for k in range(top_count):
            hit = route[k : k + 1, :] == lane_expert
            member = jnp.where(hit, 1.0, member)
            share = jnp.where(hit, route[top_count + k : top_count + k + 1, :], share)
        rank = jnp.dot(member.astype(BF16), upper, preferred_element_type=F32)
        pick = jnp.where(rank == place_in, member, 0.0)
        scaled = (share * pick).T
        coarse = scaled.astype(BF16)
        shares[b, 0] = coarse
        shares[b, 1] = (scaled - coarse.astype(F32)).astype(BF16)
        pick = pick.astype(BF16)

        def tile(j, _):
            cols = pl.ds(pl.multiple_of(j * 256, 256), 256)
            outgoing[b, :, cols] = jnp.dot(
                pick, normed[b, :, cols], preferred_element_type=F32
            ).astype(BF16)
            return 0

        lax.fori_loop(0, width // 256, tile, 0)
        exchange(outgoing, arrived, out_send, out_recv, b)

    def exchange(source, target, send, recv, b):
        mine = pl.ds(pl.multiple_of(me * capacity, capacity), capacity)

        def one(p, _):
            to = lax.rem(me + p, plane)
            pltpu.make_async_remote_copy(
                src_ref=source.at[b, pl.ds(pl.multiple_of(to * capacity, capacity), capacity)],
                dst_ref=target.at[b, mine],
                send_sem=send.at[b],
                recv_sem=recv.at[b],
                device_id=plane_dev(to),
                device_id_type=MESH,
            ).start()
            return 0

        lax.fori_loop(1, plane, one, 0)
        pltpu.make_async_copy(source.at[b, mine], target.at[b, mine], recv.at[b]).start()

    grid_rows = cos_ref.shape[0] - WINDOW
    of_row = lax.rem(lax.broadcasted_iota(jnp.int32, (WINDOW, 128), 1), HEAD_DIM) < HEAD_DIM // 2

    def angles(ref, at):
        start = lax.div(at, GRID_W)
        parts = [
            jnp.broadcast_to(ref[pl.ds(start + i, 1), :], (GRID_W, 128)) for i in range(WINDOW // GRID_W)
        ]
        return jnp.where(of_row, jnp.concatenate(parts, axis=0), ref[grid_rows:, :])

    def place(source, values, at, count):
        cosines, sines = angles(cos_ref, at), angles(sin_ref, at)
        for pair in range(kv_local // 2):
            cols = slice(pair * 128, pair * 128 + 128)
            turned = turn(source[:, cols].astype(F32), cosines, sines).astype(BF16)
            piece = values[:, cols]
            for side in range(2):
                lanes = slice(side * 64, side * 64 + 64)
                k_scr[2 * pair + side, pl.ds(at, count), :] = turned[:, lanes]
                v_scr[2 * pair + side, pl.ds(at, count), :] = piece[:, lanes]

    def place_own(i, _):
        at = pl.multiple_of(i * 128, 128)
        place(k_ref[pl.ds(at, 128), :], v_ref[pl.ds(at, 128), :], WINDOW + at, 128)
        return 0

    row = lax.rem(lax.broadcasted_iota(jnp.int32, (2 * bq, span), 0), bq)
    col = lax.broadcasted_iota(jnp.int32, (2 * bq, span), 1)
    top = lax.broadcasted_iota(jnp.int32, (2 * bq, 1), 0) < bq

    def attend(block, _):
        first = pl.multiple_of(block * bq, bq)
        cosines = angles(cos_ref, first + WINDOW) * HEAD_DIM**-0.5
        sines = angles(sin_ref, first + WINDOW) * HEAD_DIM**-0.5
        key_pos = ep * rows_here + first - WINDOW + col
        inside = (col >= row) & (col <= row + 2 * WINDOW) & (key_pos >= 0) & (key_pos < length)
        for g in range(kv_local):
            q = q_ref[pl.ds(first, bq), g * 128 : g * 128 + 128].astype(F32)
            q = turn(q, cosines, sines).astype(BF16)
            q2 = jnp.concatenate([q[:, :64], q[:, 64:]], axis=0)
            k = k_scr[g, pl.ds(first, span), :]
            v = v_scr[g, pl.ds(first, span), :]
            scores = lax.dot_general(q2, k, (((1,), (1,)), ((), ())), preferred_element_type=F32)
            scores = jnp.where(inside, scores, -jnp.inf)
            logit = jnp.where(top, sink[2 * g], sink[2 * g + 1])
            peak = jnp.maximum(jnp.max(scores, axis=1, keepdims=True), logit)
            weights = jnp.exp(scores - peak)
            total = jnp.sum(weights, axis=1, keepdims=True) + jnp.exp(logit - peak)
            chances = (weights * (1.0 / total)).astype(BF16)
            blend = jnp.dot(chances, v, preferred_element_type=F32).astype(BF16)
            att[pl.ds(first, bq), g * 128 : g * 128 + 128] = jnp.concatenate(
                [blend[:bq], blend[bq:]], axis=1
            )
        return 0

    def send_heads():
        def one(p, _):
            to = lax.rem(t + p, n_tp)
            pltpu.make_async_remote_copy(
                src_ref=att.at[pl.ds(pl.multiple_of(to * chunk, chunk), chunk)],
                dst_ref=att_in.at[t],
                send_sem=att_send,
                recv_sem=att_recv,
                device_id=(z, x, to),
                device_id_type=MESH,
            ).start()
            return 0

        lax.fori_loop(1, n_tp, one, 0)
        own = pl.ds(pl.multiple_of(t * chunk, chunk), chunk)
        pltpu.make_async_copy(att.at[own], att_in.at[t], att_recv).start()

    def experts(o):
        b = source_of(o)
        await_bytes(arrived.at[b], out_recv.at[b])
        hidden = wg.shape[1]

        def up(j, _):
            cols = pl.ds(pl.multiple_of(j * 256, 256), 256)
            rows = arrived[b]
            gate = jnp.dot(rows, wg[:, cols], preferred_element_type=F32)
            lift = jnp.dot(rows, wu[:, cols], preferred_element_type=F32)
            gate = jnp.minimum(gate, CLAMP_LIMIT)
            lift = jnp.clip(lift, -CLAMP_LIMIT, CLAMP_LIMIT)
            act[:, cols] = ((lift + 1.0) * gate * jax.nn.sigmoid(GATE_SLOPE * gate)).astype(BF16)
            return 0

        def down(j, _):
            cols = pl.ds(pl.multiple_of(j * 256, 256), 256)
            produced[b, :, cols] = jnp.dot(
                act[...], wd[:, cols], preferred_element_type=F32
            ).astype(BF16)
            return 0

        lax.fori_loop(0, hidden // 256, up, 0)
        lax.fori_loop(0, width // 256, down, 0)

    def send_back(o):
        exchange(produced, returned, back_send, back_recv, source_of(o))

    def combine(o):
        b = source_of(o)
        await_bytes(returned.at[b], back_recv.at[b])

        def tile(j, _):
            cols = pl.ds(pl.multiple_of(j * 256, 256), 256)
            rows = returned[b, :, cols]
            total = jnp.dot(shares[b, 0], rows, preferred_element_type=F32)
            total = total + jnp.dot(shares[b, 1], rows, preferred_element_type=F32)
            partial[o, :, cols] = total.astype(BF16)
            return 0

        lax.fori_loop(0, width // 256, tile, 0)
        if o > 0:
            home_copy(o).start()

    def home_copy(o):
        return pltpu.make_async_remote_copy(
            src_ref=partial.at[o],
            dst_ref=home.at[o],
            send_sem=home_send.at[o],
            recv_sem=home_recv.at[o],
            device_id=z_dev(source_of(o)),
            device_id_type=MESH,
        )

    def mixer():
        await_bytes(att_in, att_recv)
        loads[3].wait()

        def tile(j, _):
            cols = pl.ds(pl.multiple_of(j * 256, 256), 256)
            total = jnp.zeros((chunk, 256), F32)
            for s in range(n_tp):
                total = total + jnp.dot(
                    att_in[s], mix[s * width_q : s * width_q + width_q, cols], preferred_element_type=F32
                )
            mixer_ref[:, cols] = total.astype(BF16)
            return 0

        lax.fori_loop(0, width // 256, tile, 0)

    dispatch(0)
    lax.fori_loop(0, rows_here // 128, place_own, 0)
    for copy in halos:
        copy.wait()
    place(halo[0], halo[1], 0, WINDOW)
    place(halo[2], halo[3], WINDOW + rows_here, WINDOW)
    share_of = blocks // n_z
    lax.fori_loop(0, 2 * share_of, attend, 0)
    for o in range(1, 2):
        dispatch(o)
    lax.fori_loop(2 * share_of, blocks, attend, 0)
    send_heads()
    for load in loads[:3]:
        load.wait()
    experts(0)
    for o in range(2, n_z):
        dispatch(o)
        experts(o - 1)
        send_back(o - 1)
    if n_z > 2:
        combine(1)
    mixer()
    experts(n_z - 1)
    send_back(n_z - 1)
    send_back(0)
    for o in range(2 if n_z > 2 else 1, n_z):
        combine(o)
    combine(0)

    for o in range(1, n_z):
        rt_copy(o).wait_send()
        z_copy(o).wait_send()
        home_copy(o).wait()
    for b in range(n_z):
        gone = pl.ds(0, (plane - 1) * capacity)
        await_bytes(outgoing.at[b, gone], out_send.at[b])
        await_bytes(produced.at[b, gone], back_send.at[b])
    await_bytes(att.at[pl.ds(0, (n_tp - 1) * chunk)], att_send)

    for part in range(tok // 32):
        rows = slice(part * 32, part * 32 + 32)
        total = partial[0, rows, :].astype(F32)
        for o in range(1, n_z):
            total = total + home[o, rows, :].astype(F32)
        expert_ref[rows, :] = total.astype(BF16)


def body(
    queries,
    key_heads,
    value_heads,
    sink_logits,
    mix_weight,
    expert_input,
    norm_gain,
    routes,
    route_weights,
    gate_weight,
    up_weight,
    down_weight,
):
    n_z, n_x, n_tp = lax.axis_size("zz"), lax.axis_size("xx"), lax.axis_size("tp")
    n_ep = n_z * n_x
    plane = n_x * n_tp
    rows_here, width_q = queries.shape
    kv_local = key_heads.shape[1] // HEAD_DIM
    tok, top_count = routes.shape
    capacity = 2 * tok * top_count // (n_ep * n_tp)
    slots = plane * capacity
    width = expert_input.shape[1]
    hidden = gate_weight.shape[2]
    first = lax.axis_index(("zz", "xx")) * rows_here
    cosines, sines = angle_tables(first - WINDOW, rows_here + 2 * WINDOW)
    routing = jnp.concatenate([routes.astype(F32), route_weights], axis=1).T
    vmem = pl.BlockSpec(memory_space=pltpu.VMEM)
    smem = pl.BlockSpec(memory_space=pltpu.SMEM)
    anywhere = pl.BlockSpec(memory_space=pl.ANY)
    reach = rows_here + 2 * WINDOW
    dma = pltpu.SemaphoreType.DMA
    return pl.pallas_call(
        functools.partial(kernel, (n_z, n_x, n_tp, top_count, capacity)),
        in_specs=[smem] + [vmem] * 8 + [anywhere] * 4,
        out_specs=[vmem, vmem],
        out_shape=[
            jax.ShapeDtypeStruct((rows_here // n_tp, width), BF16),
            jax.ShapeDtypeStruct((tok, width), BF16),
        ],
        scratch_shapes=[
            pltpu.VMEM((kv_local, reach, HEAD_DIM), BF16),
            pltpu.VMEM((kv_local, reach, HEAD_DIM), BF16),
            pltpu.VMEM((4, WINDOW, key_heads.shape[1]), BF16),
            pltpu.VMEM((rows_here, width_q), BF16),
            pltpu.VMEM((n_tp, rows_here // n_tp, width_q), BF16),
            pltpu.VMEM((n_z, 2 * top_count, tok), F32),
            pltpu.VMEM((n_z, tok, width), BF16),
            pltpu.VMEM((n_z, slots, width), BF16),
            pltpu.VMEM((n_z, slots, width), BF16),
            pltpu.VMEM((n_z, slots, width), BF16),
            pltpu.VMEM((n_z, slots, width), BF16),
            pltpu.VMEM((n_z, 2, tok, slots), BF16),
            pltpu.VMEM((n_z, tok, width), BF16),
            pltpu.VMEM((n_z, tok, width), BF16),
            pltpu.VMEM((width, hidden), BF16),
            pltpu.VMEM((width, hidden), BF16),
            pltpu.VMEM((hidden, width), BF16),
            pltpu.VMEM(mix_weight.shape, BF16),
            pltpu.VMEM((slots, hidden), BF16),
            dma((n_z,)),
            dma((n_z,)),
            dma((n_z,)),
            dma((n_z,)),
            dma((n_z,)),
            dma((n_z,)),
            dma((n_z,)),
            dma((n_z,)),
            dma((n_z,)),
            dma((n_z,)),
            dma,
            dma,
            dma((4,)),
            dma((4,)),
            dma((4,)),
        ],
        compiler_params=pltpu.CompilerParams(
            collective_id=0, has_side_effects=True, vmem_limit_bytes=67043328
        ),
        name="layer",
    )(
        sink_logits,
        routing,
        expert_input,
        norm_gain[None, :],
        queries,
        key_heads,
        value_heads,
        cosines,
        sines,
        gate_weight,
        up_weight,
        down_weight,
        mix_weight,
    )


def z_count(mesh, n_ep):
    coords = {getattr(d, "coords", (0, 0, 0))[2] for d in mesh.devices.flat}
    return len(coords) if n_ep % len(coords) == 0 else 1


def solution(mesh):
    n_ep, n_tp = mesh.shape["ep"], mesh.shape["tp"]
    n_z = z_count(mesh, n_ep)
    grid = Mesh(mesh.devices.reshape(n_z, n_ep // n_z, n_tp), ("zz", "xx", "tp"))
    ep = ("zz", "xx")
    every = ("zz", "xx", "tp")
    return jax.shard_map(
        body,
        mesh=grid,
        in_specs=(
            P(ep, "tp"),
            P(ep, "tp"),
            P(ep, "tp"),
            P("tp"),
            P(),
            P(every, None),
            P(),
            P(every, None),
            P(every, None),
            P(every, None, None),
            P(every, None, None),
            P(every, None, None),
        ),
        out_specs=(P(every, None), P(every, None)),
        check_vma=False,
    )
```

profile of v0, /device:TPU:1, one launch (start us, length us, event | category | flops | bytes accessed | tf_op | source)
XLA Modules:
  0.0 146.4 jit_solution(4671096117902113783)
XLA Ops:
  0.7 0.1 pad_maximum_fusion
  0.8 0.7 convert_element_type.9
  1.5 1.3 maximum_bitcast_fusion.route_ref
  2.7 0.1 mul.40
  2.8 1.0 fusion
  3.8 138.4 %layer.1 = (bf16[256,2048]{1,0:T(8,128)(2,1)}, bf16[128,2048]{1,0:T(8,128)(2,1)}) custom-call(f32[8]{0:T(128)} %sink.1, f32[8,128]{1,0:T(8,128)} %maximum_bitcast_fusion.route_ref, bf16[128,2048]{1,0:T(8,128)(2,1)} %x_ref.1, f32[1,2048]{1,0:T(1,128)} %bitcast.3, bf16[1024,512]{1,0:T(8,128)(2,1)} %q_ref.1, bf16[1024,256]{1,0:T(8,128)(2,1)} %k_ref.1, ...), custom_call_target="tpu_custom_call" | custom-call | tf_op jit(solution)/shard_map/layer/pallas_call | solution.py:490
  142.2 2.3 %copy.16 = bf16[256,2048]{1,0:T(8,128)(2,1)} copy(bf16[256,2048]{1,0:T(8,128)(2,1)} %get-tuple-element.6) | data formatting | bytes 2097152
  144.5 1.9 %copy.17 = bf16[128,2048]{1,0:T(8,128)(2,1)} copy(bf16[128,2048]{1,0:T(8,128)(2,1)} %get-tuple-element.7) | data formatting | bytes 1048576
  (5 shorter events, 0.0 us)
where the time goes:
time: 149 us; the launch traced here: 146 us
  Pallas kernels  138 us (93%)
  local copies, waits for them, and re-layouts  4.27 us (3%)
  other arithmetic  3.09 us (2%)
    pallas_call x1, Pallas kernels, body(): pl.pallas_call(functools.partial(kernel, (n_z, n_x, n_tp, top_count, capa...  138 us
    unnamed x2, local copies, waits for them, and re-layouts  4.18 us

commit v1 on v0

v1 whole, which is shorter than its diff:
```python
import functools

import jax
import jax.numpy as jnp
import numpy as np
from jax import lax
from jax.experimental import pallas as pl
from jax.experimental.pallas import tpu as pltpu
from jax.sharding import Mesh
from jax.sharding import PartitionSpec as P

HEAD_DIM = 64
WINDOW = 128
GRID_W = 64
ROPE_BASE = 10000.0
CLAMP_LIMIT = 7.0
GATE_SLOPE = 1.702
NORM_EPS = 1e-05

F32 = jnp.float32
BF16 = jnp.bfloat16
MESH = pl.DeviceIdType.MESH
PANELS = 2
TILE = 256

scope = jax.named_scope


def table_rows(rows_here):
    return -(-(rows_here + 2 * WINDOW) // GRID_W // 8) * 8


def angle_tables(length, rows_here):
    half = HEAD_DIM // 2
    quarter = HEAD_DIM // 4
    lane = np.arange(2 * HEAD_DIM) % HEAD_DIM
    freqs = (ROPE_BASE ** (-np.arange(0, half, 2) / half)).astype(np.float32)
    lane_freq = np.tile(freqs, 2 * HEAD_DIM // quarter)
    count = (length - rows_here) // GRID_W + table_rows(rows_here)
    by_row = np.arange(count) - WINDOW // GRID_W
    by_col = np.arange(WINDOW) % GRID_W
    place = np.concatenate([by_row, by_col]).astype(np.float32)
    angle = (place[:, None] * lane_freq[None, :]).astype(np.float64)
    sign = np.where(lane % half < quarter, -1.0, 1.0)
    return np.stack([np.cos(angle), np.sin(angle) * sign]).astype(np.float32)


def turn(cells, cosines, sines):
    quarter = HEAD_DIM // 4
    width = cells.shape[1]
    lane = lax.broadcasted_iota(jnp.int32, cells.shape, 1)
    ahead = pltpu.roll(cells, width - quarter, 1)
    behind = pltpu.roll(cells, quarter, 1)
    partner = jnp.where(lane % (2 * quarter) < quarter, ahead, behind)
    return cells * cosines + partner * sines

def kernel(
    sizes,
    sink_hbm,
    route_hbm,
    share_hbm,
    x_hbm,
    gain_hbm,
    q_hbm,
    k_hbm,
    v_hbm,
    table_hbm,
    wg_hbm,
    wu_hbm,
    wd_hbm,
    mix_hbm,
    mixer_hbm,
    expert_hbm,
    sink,
    route_ref,
    share_ref,
    x_ref,
    gain_ref,
    q_ref,
    k_ref,
    v_ref,
    by_row,
    by_col,
    mixer_ref,
    expert_ref,
    k_scr,
    v_scr,
    halo,
    att,
    att_in,
    routing,
    normed,
    picks,
    outgoing,
    arrived,
    produced,
    returned,
    shares,
    partial,
    home,
    wg,
    wu,
    wd,
    mix,
    act,
    z_send,
    z_recv,
    rt_send,
    rt_recv,
    out_send,
    out_recv,
    back_send,
    back_recv,
    home_send,
    home_recv,
    att_send,
    att_recv,
    halo_send,
    halo_recv,
    load_sem,
):
    n_z, n_x, n_tp, top_count, capacity = sizes
    n_ep = n_z * n_x
    plane = n_x * n_tp
    slots = plane * capacity
    z, x, t = lax.axis_index("zz"), lax.axis_index("xx"), lax.axis_index("tp")
    me = x * n_tp + t
    ep = z * n_x + x
    rows_here, width_q = q_ref.shape
    tok, width = x_ref.shape
    panel = width // PANELS
    length = rows_here * n_ep
    kv_local = k_scr.shape[0]
    bq = WINDOW
    span = bq + 2 * WINDOW
    blocks = rows_here // bq
    chunk = rows_here // n_tp
    last = n_z - 1
    grid_rows = by_row.shape[1]
    table_end = table_hbm.shape[1] - WINDOW

    def z_dev(b):
        return (b, x, t)

    def plane_dev(p):
        return (z, lax.div(p, n_tp), lax.rem(p, n_tp))

    def ep_dev(e):
        return (lax.div(e, n_x), lax.rem(e, n_x), t)

    after, before = lax.rem(ep + 1, n_ep), lax.rem(ep + n_ep - 1, n_ep)
    has_after, has_before = ep < n_ep - 1, ep > 0
    has_up, has_down = z < last, z > 0
    end = (z == 0) | (z == last)
    mid = (z > 0) & (z < last)

    closer = jnp.minimum(z, last - z)
    far_side = jnp.where(z < last - z, 1, -1)

    def nearest(i):
        if i == 0:
            return z
        paired = z + ((i + 1) // 2) * (-1 if i % 2 else 1)
        return jnp.where(i <= 2 * closer, paired, z + far_side * (i - closer))

    def going_back(i):
        return lax.bitwise_xor(z, jnp.int32(last - i))

    first_row = pl.multiple_of(ep * (rows_here // GRID_W), 8)
    loads = {
        "x": (x_hbm, x_ref),
        "gain": (gain_hbm, gain_ref),
        "route": (route_hbm, route_ref),
        "share": (share_hbm, share_ref),
        "sink": (sink_hbm, sink),
        "k": (k_hbm, k_ref),
        "v": (v_hbm, v_ref),
        "by_row": (table_hbm.at[:, pl.ds(first_row, grid_rows)], by_row),
        "by_col": (table_hbm.at[:, pl.ds(table_end, WINDOW)], by_col),
        "q": (q_hbm, q_ref),
        "wg": (wg_hbm.at[0], wg),
        "wu": (wu_hbm.at[0], wu),
        "wd": (wd_hbm.at[0], wd),
        "mix": (mix_hbm, mix),
    }
    loads = {
        name: pltpu.make_async_copy(source, target, load_sem.at[i])
        for i, (name, (source, target)) in enumerate(loads.items())
    }
    for load in loads.values():
        load.start()

    def loaded(*names):
        for name in names:
            loads[name].wait()

    barrier = pltpu.get_barrier_semaphore()

    def greet_z(o, _):
        pl.semaphore_signal(barrier, inc=1, device_id=z_dev(lax.rem(z + o, n_z)), device_id_type=MESH)
        return 0

    def greet_plane(p, _):
        pl.semaphore_signal(
            barrier, inc=1, device_id=plane_dev(lax.rem(me + p, plane)), device_id_type=MESH
        )
        return 0

    lax.fori_loop(1, n_z, greet_z, 0)
    lax.fori_loop(1, plane, greet_plane, 0)
    for e in (after, before):
        pl.semaphore_signal(barrier, inc=1, device_id=ep_dev(e), device_id_type=MESH)

    loaded("x", "gain")
    with scope("norm"):
        for part in range(tok // 32):
            rows = slice(part * 32, part * 32 + 32)
            values = x_ref[rows, :].astype(F32)
            center = jnp.mean(values, axis=1, keepdims=True)
            spread = jnp.mean(jnp.square(values - center), axis=1, keepdims=True)
            result = ((values - center) * lax.rsqrt(spread + NORM_EPS) * gain_ref[...]).astype(BF16)
            for h in range(PANELS):
                normed[z, h, rows, :] = result[:, h * panel : h * panel + panel]
    loaded("route", "share")
    routing[z, :top_count, :] = route_ref[...].astype(F32)
    routing[z, top_count:, :] = share_ref[...]
    with scope("barr"):
        pl.semaphore_wait(barrier, n_z - 1 + plane - 1 + 2)

    def rt_copy(o):
        return pltpu.make_async_remote_copy(
            src_ref=routing.at[z],
            dst_ref=routing.at[z],
            send_sem=rt_send.at[o],
            recv_sem=rt_recv.at[z],
            device_id=z_dev(lax.rem(z + o, n_z)),
            device_id_type=MESH,
        )

    def z_copy(i, h, b, target):
        return pltpu.make_async_remote_copy(
            src_ref=normed.at[b, h],
            dst_ref=normed.at[b, h],
            send_sem=z_send.at[i, h],
            recv_sem=z_recv.at[b, h],
            device_id=z_dev(target),
            device_id_type=MESH,
        )

    def onward(i):
        b = nearest(i)
        target = jnp.where(b < z, z + 1, z - 1)
        return b, target, (target >= 0) & (target <= last)

    for o in range(1, n_z):
        rt_copy(o).start()
    if n_z > 1:
        for h in range(PANELS):

            @pl.when(has_up)
            def _():
                z_copy(0, h, z, z + 1).start()

            @pl.when(has_down)
            def _():
                z_copy(n_z, h, z, z - 1).start()

    def await_bytes(ref, sem):
        pltpu.make_async_copy(ref, ref, sem).wait()

    def tick(distance, h):
        for i in range(1, n_z):
            if not (i + 1) // 2 <= distance <= i:
                continue
            b, target, goes_on = onward(i)

            @pl.when(jnp.abs(b - z) == distance)
            def _():
                with scope(f"zwait{i}{h}"):
                    await_bytes(normed.at[b, h], z_recv.at[b, h])

                @pl.when(goes_on)
                def _():
                    z_copy(i, h, b, target).start()

    slot_row = lax.broadcasted_iota(jnp.int32, (slots, tok), 0)

    def choose(i):
        b = nearest(i)
        if i > 0:
            await_bytes(routing.at[b], rt_recv.at[b])
        lane_expert = (z * plane + lax.div(slot_row, capacity)).astype(F32)
        place_in = lax.rem(slot_row, capacity).astype(F32)
        upper = (
            lax.broadcasted_iota(jnp.int32, (tok, tok), 0) < lax.broadcasted_iota(jnp.int32, (tok, tok), 1)
        ).astype(F32).astype(BF16)
        route = routing[b]
        member = jnp.zeros((slots, tok), F32)
        share = jnp.zeros((slots, tok), F32)
        for k in range(top_count):
            hit = route[k : k + 1, :] == lane_expert
            member = jnp.where(hit, 1.0, member)
            share = jnp.where(hit, route[top_count + k : top_count + k + 1, :], share)
        rank = jnp.dot(member.astype(BF16), upper, preferred_element_type=F32)
        pick = jnp.where(rank == place_in, member, 0.0)
        picks[...] = pick.astype(BF16)
        scaled = (share * pick).T
        coarse = scaled.astype(BF16)
        shares[b, 0] = coarse
        shares[b, 1] = (scaled - coarse.astype(F32)).astype(BF16)

    def dispatch(i, h):
        b = nearest(i)
        with scope(f"disp{i}{h}"):
            if h == 0:
                choose(i)

            def tile(j, _):
                cols = pl.ds(pl.multiple_of(j * TILE, TILE), TILE)
                outgoing[b, h, :, cols] = jnp.dot(
                    picks[...], normed[b, h, :, cols], preferred_element_type=F32
                ).astype(BF16)
                return 0

            lax.fori_loop(0, panel // TILE, tile, 0)
            exchange(outgoing, arrived, out_send, out_recv, b, h)

    def exchange(source, target, send, recv, b, h):
        mine = pl.ds(pl.multiple_of(me * capacity, capacity), capacity)

        def one(p, _):
            to = lax.rem(me + p, plane)
            pltpu.make_async_remote_copy(
                src_ref=source.at[b, h, pl.ds(pl.multiple_of(to * capacity, capacity), capacity)],
                dst_ref=target.at[b, h, mine],
                send_sem=send.at[b, h],
                recv_sem=recv.at[b, h],
                device_id=plane_dev(to),
                device_id_type=MESH,
            ).start()
            return 0

        lax.fori_loop(1, plane, one, 0)
        pltpu.make_async_copy(source.at[b, h, mine], target.at[b, h, mine], recv.at[b, h]).start()

    def halo_copy(source, which, start, target):
        return pltpu.make_async_remote_copy(
            src_ref=source.at[pl.ds(start, WINDOW)],
            dst_ref=halo.at[which],
            send_sem=halo_send.at[which],
            recv_sem=halo_recv.at[which],
            device_id=ep_dev(target),
            device_id_type=MESH,
        )

    to_after = [
        halo_copy(k_ref, 0, rows_here - WINDOW, after),
        halo_copy(v_ref, 1, rows_here - WINDOW, after),
    ]
    to_before = [halo_copy(k_ref, 2, 0, before), halo_copy(v_ref, 3, 0, before)]

    def send_halos():
        for there, copies in ((has_after, to_after), (has_before, to_before)):

            @pl.when(there)
            def _():
                for copy in copies:
                    copy.start()

    def await_halos():
        for there, copies in ((has_before, to_after), (has_after, to_before)):

            @pl.when(there)
            def _():
                for copy in copies:
                    copy.wait_recv()

        for there, which in ((has_before, 0), (has_after, 2)):

            @pl.when(jnp.logical_not(there))
            def _():
                halo[which] = jnp.zeros(halo.shape[1:], BF16)
                halo[which + 1] = jnp.zeros(halo.shape[1:], BF16)

    of_row = lax.rem(lax.broadcasted_iota(jnp.int32, (WINDOW, 128), 1), HEAD_DIM) < HEAD_DIM // 2

    def angles(which, at):
        start = lax.div(at, GRID_W)
        parts = [
            jnp.broadcast_to(by_row[which, pl.ds(start + i, 1), :], (GRID_W, 128))
            for i in range(WINDOW // GRID_W)
        ]
        return jnp.where(of_row, jnp.concatenate(parts, axis=0), by_col[which])

    def place(source, values, at, count):
        cosines, sines = angles(0, at), angles(1, at)
        for pair in range(kv_local // 2):
            cols = slice(pair * 128, pair * 128 + 128)
            turned = turn(source[:, cols].astype(F32), cosines, sines).astype(BF16)
            piece = values[:, cols]
            for side in range(2):
                lanes = slice(side * 64, side * 64 + 64)
                k_scr[2 * pair + side, pl.ds(at, count), :] = turned[:, lanes]
                v_scr[2 * pair + side, pl.ds(at, count), :] = piece[:, lanes]

    def place_own(i, _):
        at = pl.multiple_of(i * 128, 128)
        place(k_ref[pl.ds(at, 128), :], v_ref[pl.ds(at, 128), :], WINDOW + at, 128)
        return 0

    row = lax.rem(lax.broadcasted_iota(jnp.int32, (2 * bq, span), 0), bq)
    col = lax.broadcasted_iota(jnp.int32, (2 * bq, span), 1)
    top = lax.broadcasted_iota(jnp.int32, (2 * bq, 1), 0) < bq

    def attend(block, _):
        first = pl.multiple_of(block * bq, bq)
        cosines = angles(0, first + WINDOW) * HEAD_DIM**-0.5
        sines = angles(1, first + WINDOW) * HEAD_DIM**-0.5
        key_pos = ep * rows_here + first - WINDOW + col
        inside = (col >= row) & (col <= row + 2 * WINDOW) & (key_pos >= 0) & (key_pos < length)
        for g in range(kv_local):
            q = q_ref[pl.ds(first, bq), g * 128 : g * 128 + 128].astype(F32)
            q = turn(q, cosines, sines).astype(BF16)
            q2 = jnp.concatenate([q[:, :64], q[:, 64:]], axis=0)
            k = k_scr[g, pl.ds(first, span), :]
            v = v_scr[g, pl.ds(first, span), :]
            scores = lax.dot_general(q2, k, (((1,), (1,)), ((), ())), preferred_element_type=F32)
            scores = jnp.where(inside, scores, -jnp.inf)
            logit = jnp.where(top, sink[2 * g], sink[2 * g + 1])
            peak = jnp.maximum(jnp.max(scores, axis=1, keepdims=True), logit)
            weights = jnp.exp(scores - peak)
            total = jnp.sum(weights, axis=1, keepdims=True) + jnp.exp(logit - peak)
            chances = (weights * (1.0 / total)).astype(BF16)
            blend = jnp.dot(chances, v, preferred_element_type=F32).astype(BF16)
            att[pl.ds(first, bq), g * 128 : g * 128 + 128] = jnp.concatenate(
                [blend[:bq], blend[bq:]], axis=1
            )
        return 0

    def attend_inner(part, parts):
        inner = blocks - 2
        with scope(f"att{part}"):
            lax.fori_loop(1 + inner * part // parts, 1 + inner * (part + 1) // parts, attend, 0)

    def attend_edges():
        with scope("halowait"):
            await_halos()
        with scope("edges"):
            place(halo[0], halo[1], 0, WINDOW)
            place(halo[2], halo[3], WINDOW + rows_here, WINDOW)
            lax.fori_loop(0, 2, lambda i, _: attend(i * (blocks - 1), _), 0)

    def send_heads():
        def one(p, _):
            to = lax.rem(t + p, n_tp)
            pltpu.make_async_remote_copy(
                src_ref=att.at[pl.ds(pl.multiple_of(to * chunk, chunk), chunk)],
                dst_ref=att_in.at[t],
                send_sem=att_send,
                recv_sem=att_recv,
                device_id=(z, x, to),
                device_id_type=MESH,
            ).start()
            return 0

        lax.fori_loop(1, n_tp, one, 0)
        own = pl.ds(pl.multiple_of(t * chunk, chunk), chunk)
        pltpu.make_async_copy(att.at[own], att_in.at[t], att_recv).start()

    mixer_out = pltpu.make_async_copy(mixer_ref, mixer_hbm, load_sem.at[len(loads)])

    def mixer():
        with scope("attwait"):
            await_bytes(att_in, att_recv)
        loaded("mix")

        def tile(j, _):
            cols = pl.ds(pl.multiple_of(j * TILE, TILE), TILE)
            total = jnp.zeros((chunk, TILE), F32)
            for s in range(n_tp):
                total = total + jnp.dot(
                    att_in[s], mix[s * width_q : s * width_q + width_q, cols], preferred_element_type=F32
                )
            mixer_ref[:, cols] = total.astype(BF16)
            return 0

        with scope("mixer"):
            lax.fori_loop(0, width // TILE, tile, 0)
        mixer_out.start()

    def experts(i, sent=lambda h: None):
        b = nearest(i)
        hidden = wg.shape[1]
        for h in range(PANELS):
            with scope(f"arrwait{i}{h}"):
                await_bytes(arrived.at[b, h], out_recv.at[b, h])

        def up(j, _):
            cols = pl.ds(pl.multiple_of(j * TILE, TILE), TILE)
            gate = jnp.zeros((slots, TILE), F32)
            lift = jnp.zeros((slots, TILE), F32)
            for h in range(PANELS):
                rows = arrived[b, h]
                deep = slice(h * panel, h * panel + panel)
                gate = gate + jnp.dot(rows, wg[deep, cols], preferred_element_type=F32)
                lift = lift + jnp.dot(rows, wu[deep, cols], preferred_element_type=F32)
            gate = jnp.minimum(gate, CLAMP_LIMIT)
            lift = jnp.clip(lift, -CLAMP_LIMIT, CLAMP_LIMIT)
            act[:, cols] = ((lift + 1.0) * gate * jax.nn.sigmoid(GATE_SLOPE * gate)).astype(BF16)
            return 0

        with scope(f"exp{i}"):
            lax.fori_loop(0, hidden // TILE, up, 0)
            for h in range(PANELS):

                def down(j, _):
                    cols = pl.ds(pl.multiple_of(j * TILE, TILE), TILE)
                    wide = pl.ds(pl.multiple_of(h * panel + j * TILE, TILE), TILE)
                    produced[b, h, :, cols] = jnp.dot(
                        act[...], wd[:, wide], preferred_element_type=F32
                    ).astype(BF16)
                    return 0

                lax.fori_loop(0, panel // TILE, down, 0)
                sent(h)

    def send_back(b, h):
        exchange(produced, returned, back_send, back_recv, b, h)

    def home_copy(b, h):
        target = jnp.where(b < z, z - 1, z + 1)
        slot = jnp.where((target == b) & (b < z), n_z, b)
        return pltpu.make_async_remote_copy(
            src_ref=partial.at[b, h],
            dst_ref=home.at[slot, h],
            send_sem=home_send.at[b, h],
            recv_sem=home_recv.at[slot, h],
            device_id=z_dev(target),
            device_id_type=MESH,
        )

    def clear_home():
        for slot in range(n_z + 1):
            from_up = (slot < z) | (slot == n_z)
            missing = jnp.where(from_up, z == last, z == 0)

            @pl.when(missing)
            def _():
                home[slot] = jnp.zeros(home.shape[1:], BF16)

    def weighted(b, h, cols):
        rows = returned[b, h, :, cols]
        total = jnp.dot(shares[b, 0], rows, preferred_element_type=F32)
        return total + jnp.dot(shares[b, 1], rows, preferred_element_type=F32)

    def combine(name, b, h):
        with scope(f"retwait{name}{h}"):
            await_bytes(returned.at[b, h], back_recv.at[b, h])

        @pl.when(mid)
        def _():
            with scope(f"chain{name}{h}"):
                await_bytes(home.at[b, h], home_recv.at[b, h])

        def tile(j, _):
            cols = pl.ds(pl.multiple_of(j * TILE, TILE), TILE)
            total = weighted(b, h, cols) + home[b, h, :, cols].astype(F32)
            partial[b, h, :, cols] = total.astype(BF16)
            return 0

        with scope(f"comb{name}{h}"):
            lax.fori_loop(0, panel // TILE, tile, 0)
        home_copy(b, h).start()

    expert_out = [
        pltpu.make_async_copy(
            expert_ref.at[:, pl.ds(h * panel, panel)],
            expert_hbm.at[:, pl.ds(h * panel, panel)],
            load_sem.at[len(loads) + 1 + h],
        )
        for h in range(PANELS)
    ]

    def combine_own(h):
        with scope(f"retwaitown{h}"):
            await_bytes(returned.at[z, h], back_recv.at[z, h])

        with scope(f"homewait{h}"):

            @pl.when(has_down)
            def _():
                await_bytes(home.at[z, h], home_recv.at[z, h])

            @pl.when(has_up)
            def _():
                await_bytes(home.at[n_z, h], home_recv.at[n_z, h])

        def tile(j, _):
            cols = pl.ds(pl.multiple_of(j * TILE, TILE), TILE)
            wide = pl.ds(pl.multiple_of(h * panel + j * TILE, TILE), TILE)
            total = weighted(z, h, cols) + home[z, h, :, cols].astype(F32)
            total = total + home[n_z, h, :, cols].astype(F32)
            expert_ref[:, wide] = total.astype(BF16)
            return 0

        with scope(f"combown{h}"):
            lax.fori_loop(0, panel // TILE, tile, 0)
        expert_out[h].start()

    for h in range(PANELS):
        dispatch(0, h)
    clear_home()
    loaded("k", "v", "by_row", "by_col", "q", "sink")
    with scope("place"):
        lax.fori_loop(0, rows_here // 128, place_own, 0)
    attend_inner(0, 3)
    for h in range(PANELS):
        if n_z > 1:
            tick(1, h)
            dispatch(1, h)
        attend_inner(1 + h, 3)
    if n_z > 2:
        tick(2, 0)
        dispatch(2, 0)
    loaded("wg", "wu", "wd")
    if n_z == 1:
        send_halos()
    if n_z > 1:
        experts(0)
    if n_z > 2:
        tick(2, 1)
        dispatch(2, 1)
    if n_z > 1:
        send_halos()
    if n_z > 2:
        experts(1)
        for h in range(PANELS):
            tick(3, h)
            dispatch(3, h)
        experts(2)
    attend_edges()
    send_heads()
    if n_z > 2:

        @pl.when(mid)
        def _():
            for h in range(PANELS):
                send_back(going_back(0), h)

    def sent(h):
        @pl.when(end)
        def _():
            send_back(going_back(0), h)

    experts(last, sent)
    for i in range(1, n_z):
        for h in range(PANELS):
            send_back(going_back(i), h)
    mixer()
    for i in range(last):
        b = going_back(i)
        if n_z > 2:
            b = jnp.where(mid, going_back((i + 1) % last), b)
        for h in range(PANELS):
            combine(i, b, h)
    for h in range(PANELS):
        combine_own(h)

    for o in range(1, n_z):
        rt_copy(o).wait_send()
    if n_z > 1:
        for h in range(PANELS):

            @pl.when(has_up)
            def _():
                z_copy(0, h, z, z + 1).wait_send()

            @pl.when(has_down)
            def _():
                z_copy(n_z, h, z, z - 1).wait_send()

            for i in range(1, n_z):
                b, target, goes_on = onward(i)

                @pl.when(goes_on)
                def _():
                    z_copy(i, h, b, target).wait_send()

                home_copy(b, h).wait_send()
    for there, copies in ((has_after, to_after), (has_before, to_before)):

        @pl.when(there)
        def _():
            for copy in copies:
                copy.wait_send()

    for b in range(n_z):
        for h in range(PANELS):
            gone = pl.ds(0, (plane - 1) * capacity)
            await_bytes(outgoing.at[b, h, gone], out_send.at[b, h])
            await_bytes(produced.at[b, h, gone], back_send.at[b, h])
    await_bytes(att.at[pl.ds(0, (n_tp - 1) * chunk)], att_send)
    mixer_out.wait()
    for copy in expert_out:
        copy.wait()


def hand_over(mixer_in, expert_in, mixer_out, expert_out, mixer_scr, expert_scr, sem):
    steps = []
    for source, scratch, target, at, parts in (
        (mixer_in, mixer_scr, mixer_out, 0, 4),
        (expert_in, expert_scr, expert_out, 4, 2),
    ):
        rows = source.shape[0] // parts
        for part in range(parts):
            here = pl.ds(part * rows, rows)
            steps.append(
                (
                    pltpu.make_async_copy(source.at[here], scratch.at[here], sem.at[0, at + part]),
                    pltpu.make_async_copy(scratch.at[here], target.at[here], sem.at[1, at + part]),
                )
            )
    for take, _ in steps:
        take.start()
    for take, give in steps:
        take.wait()
        give.start()
    for _, give in steps:
        give.wait()


def body(
    queries,
    key_heads,
    value_heads,
    sink_logits,
    mix_weight,
    expert_input,
    norm_gain,
    routes,
    route_weights,
    gate_weight,
    up_weight,
    down_weight,
):
    n_z, n_x, n_tp = lax.axis_size("zz"), lax.axis_size("xx"), lax.axis_size("tp")
    n_ep = n_z * n_x
    plane = n_x * n_tp
    rows_here, width_q = queries.shape
    kv_width = key_heads.shape[1]
    kv_local = kv_width // HEAD_DIM
    tok, top_count = routes.shape
    capacity = 2 * tok * top_count // (n_ep * n_tp)
    slots = plane * capacity
    width = expert_input.shape[1]
    panel = width // PANELS
    hidden = gate_weight.shape[2]
    tables = jnp.asarray(angle_tables(rows_here * n_ep, rows_here))
    anywhere = pl.BlockSpec(memory_space=pl.ANY)
    reach = rows_here + 2 * WINDOW
    dma = pltpu.SemaphoreType.DMA
    shapes = [
        jax.ShapeDtypeStruct((rows_here // n_tp, width), BF16),
        jax.ShapeDtypeStruct((tok, width), BF16),
    ]
    both = dma((n_z, PANELS))
    mixed, expert = pl.pallas_call(
        functools.partial(kernel, (n_z, n_x, n_tp, top_count, capacity)),
        in_specs=[anywhere] * 13,
        out_specs=[anywhere] * 2,
        out_shape=shapes,
        scratch_shapes=[
            pltpu.SMEM(sink_logits.shape, F32),
            pltpu.VMEM((top_count, tok), jnp.int32),
            pltpu.VMEM((top_count, tok), F32),
            pltpu.VMEM((tok, width), BF16),
            pltpu.VMEM((1, width), F32),
            pltpu.VMEM((rows_here, width_q), BF16),
            pltpu.VMEM((rows_here, kv_width), BF16),
            pltpu.VMEM((rows_here, kv_width), BF16),
            pltpu.VMEM((2, table_rows(rows_here), 128), F32),
            pltpu.VMEM((2, WINDOW, 128), F32),
            pltpu.VMEM((rows_here // n_tp, width), BF16),
            pltpu.VMEM((tok, width), BF16),
            pltpu.VMEM((kv_local, reach, HEAD_DIM), BF16),
            pltpu.VMEM((kv_local, reach, HEAD_DIM), BF16),
            pltpu.VMEM((4, WINDOW, kv_width), BF16),
            pltpu.VMEM((rows_here, width_q), BF16),
            pltpu.VMEM((n_tp, rows_here // n_tp, width_q), BF16),
            pltpu.VMEM((n_z, 2 * top_count, tok), F32),
            pltpu.VMEM((n_z, PANELS, tok, panel), BF16),
            pltpu.VMEM((slots, tok), BF16),
            pltpu.VMEM((n_z, PANELS, slots, panel), BF16),
            pltpu.VMEM((n_z, PANELS, slots, panel), BF16),
            pltpu.VMEM((n_z, PANELS, slots, panel), BF16),
            pltpu.VMEM((n_z, PANELS, slots, panel), BF16),
            pltpu.VMEM((n_z, 2, tok, slots), BF16),
            pltpu.VMEM((n_z, PANELS, tok, panel), BF16),
            pltpu.VMEM((n_z + 1, PANELS, tok, panel), BF16),
            pltpu.VMEM((width, hidden), BF16),
            pltpu.VMEM((width, hidden), BF16),
            pltpu.VMEM((hidden, width), BF16),
            pltpu.VMEM(mix_weight.shape, BF16),
            pltpu.VMEM((slots, hidden), BF16),
            dma((n_z + 1, PANELS)),
            both,
            dma((n_z,)),
            dma((n_z,)),
            both,
            both,
            both,
            both,
            both,
            dma((n_z + 1, PANELS)),
            dma,
            dma,
            dma((4,)),
            dma((4,)),
            dma((15 + PANELS,)),
        ],
        compiler_params=pltpu.CompilerParams(
            collective_id=0, has_side_effects=True, vmem_limit_bytes=67043328
        ),
        name="layer",
    )(
        sink_logits,
        routes.T,
        route_weights.T,
        expert_input,
        norm_gain[None, :],
        queries,
        key_heads,
        value_heads,
        tables,
        gate_weight,
        up_weight,
        down_weight,
        mix_weight,
    )
    return pl.pallas_call(
        hand_over,
        in_specs=[anywhere] * 2,
        out_specs=[anywhere] * 2,
        out_shape=shapes,
        scratch_shapes=[pltpu.VMEM(s.shape, BF16) for s in shapes] + [dma((2, 6))],
        name="hand_over",
    )(mixed, expert)


def z_count(mesh, n_ep):
    coords = {getattr(d, "coords", (0, 0, 0))[2] for d in mesh.devices.flat}
    return len(coords) if len(coords) in (2, 4) and n_ep % len(coords) == 0 else 1


def solution(mesh):
    n_ep, n_tp = mesh.shape["ep"], mesh.shape["tp"]
    n_z = z_count(mesh, n_ep)
    grid = Mesh(mesh.devices.reshape(n_z, n_ep // n_z, n_tp), ("zz", "xx", "tp"))
    ep = ("zz", "xx")
    every = ("zz", "xx", "tp")
    return jax.shard_map(
        body,
        mesh=grid,
        in_specs=(
            P(ep, "tp"),
            P(ep, "tp"),
            P(ep, "tp"),
            P("tp"),
            P(),
            P(every, None),
            P(),
            P(every, None),
            P(every, None),
            P(every, None, None),
            P(every, None, None),
            P(every, None, None),
        ),
        out_specs=(P(every, None), P(every, None)),
        check_vma=False,
    )
```

time: 149 us -> 125 us (0.84)
  Pallas kernels: 138 us -> 122 us
  local copies, waits for them, and re-layouts: 4.27 us -> 0 us
  other arithmetic: 3.09 us -> 0 us
    pallas_call x1, Pallas kernels: 138 us -> 120 us  [body(): pl.pallas_call(functools.partial(kernel, (n_z, n_x, n_tp, top_count, capa...]
    unnamed x2 -> x0, local copies, waits for them, and re-layouts: 4.18 us -> none
    pallas_call x0 -> x1, Pallas kernels: none -> 2.19 us  [body(): pl.pallas_call(hand_over, in_specs=[anywhere] * 2, out_specs=[anywhere] *...]
where the time goes in v1:
time: 125 us; the launch traced here: 123 us
  Pallas kernels  122 us (98%)
    pallas_call x1, Pallas kernels, body(): pl.pallas_call(functools.partial(kernel, (n_z, n_x, n_tp, top_count, capa...  120 us

profile of v1, /device:TPU:1, one launch (start us, length us, event | category | flops | bytes accessed | tf_op | source)
XLA Modules:
  0.0 123.0 jit_solution(9447274235509611457)
XLA Ops:
  0.6 120.2 %layer.1 = (bf16[256,2048]{1,0:T(8,128)(2,1)}, bf16[128,2048]{1,0:T(8,128)(2,1)}) custom-call(f32[8]{0:T(128)} %sink_hbm.1, s32[4,128]{1,0:T(4,128)} %bitcast.4, f32[4,128]{1,0:T(4,128)} %bitcast.5, bf16[128,2048]{1,0:T(8,128)(2,1)} %x_hbm.1, f32[1,2048]{1,0:T(1,128)} %bitcast.3, bf16[1024,512]{1,0:T(8,128)(2,1)} %q_hbm.1, bf16[1024,256]{1,0:T(8,128)(2,1)} %k_hbm.1, ...), custom_call_target="tpu_custom_call" | custom-call | tf_op jit(solution)/shard_map/layer/pallas_call | solution.py:767
  120.8 2.2 %hand_over.1 = (bf16[256,2048]{1,0:T(8,128)(2,1)}, bf16[128,2048]{1,0:T(8,128)(2,1)}) custom-call(bf16[256,2048]{1,0:T(8,128)(2,1)} %get-tuple-element.4.mixer_in, bf16[128,2048]{1,0:T(8,128)(2,1)} %get-tuple-element.5.expert_in), custom_call_target="tpu_custom_call" | custom-call | tf_op jit(solution)/shard_map/hand_over/pallas_call | solution.py:840

commit v2 on v1

--- a/solution.py
+++ b/solution.py
@@ -22,6 +22,7 @@
 MESH = pl.DeviceIdType.MESH
 PANELS = 2
 TILE = 256
+VMEM_BYTES = 61 << 20
 
 scope = jax.named_scope
 
@@ -69,8 +70,8 @@
     wu_hbm,
     wd_hbm,
     mix_hbm,
-    mixer_hbm,
-    expert_hbm,
+    mixer_ref,
+    expert_ref,
     sink,
     route_ref,
     share_ref,
@@ -81,8 +82,6 @@
     v_ref,
     by_row,
     by_col,
-    mixer_ref,
-    expert_ref,
     k_scr,
     v_scr,
     halo,
@@ -168,10 +167,10 @@
 
     first_row = pl.multiple_of(ep * (rows_here // GRID_W), 8)
     loads = {
+        "route": (route_hbm, route_ref),
+        "share": (share_hbm, share_ref),
         "x": (x_hbm, x_ref),
         "gain": (gain_hbm, gain_ref),
-        "route": (route_hbm, route_ref),
-        "share": (share_hbm, share_ref),
         "sink": (sink_hbm, sink),
         "k": (k_hbm, k_ref),
         "v": (v_hbm, v_ref),
@@ -211,77 +210,8 @@
     for e in (after, before):
         pl.semaphore_signal(barrier, inc=1, device_id=ep_dev(e), device_id_type=MESH)
 
-    loaded("x", "gain")
-    with scope("norm"):
-        for part in range(tok // 32):
-            rows = slice(part * 32, part * 32 + 32)
-            values = x_ref[rows, :].astype(F32)
-            center = jnp.mean(values, axis=1, keepdims=True)
-            spread = jnp.mean(jnp.square(values - center), axis=1, keepdims=True)
-            result = ((values - center) * lax.rsqrt(spread + NORM_EPS) * gain_ref[...]).astype(BF16)
-            for h in range(PANELS):
-                normed[z, h, rows, :] = result[:, h * panel : h * panel + panel]
-    loaded("route", "share")
-    routing[z, :top_count, :] = route_ref[...].astype(F32)
-    routing[z, top_count:, :] = share_ref[...]
-    with scope("barr"):
-        pl.semaphore_wait(barrier, n_z - 1 + plane - 1 + 2)
-
-    def rt_copy(o):
-        return pltpu.make_async_remote_copy(
-            src_ref=routing.at[z],
-            dst_ref=routing.at[z],
-            send_sem=rt_send.at[o],
-            recv_sem=rt_recv.at[z],
-            device_id=z_dev(lax.rem(z + o, n_z)),
-            device_id_type=MESH,
-        )
-
-    def z_copy(i, h, b, target):
-        return pltpu.make_async_remote_copy(
-            src_ref=normed.at[b, h],
-            dst_ref=normed.at[b, h],
-            send_sem=z_send.at[i, h],
-            recv_sem=z_recv.at[b, h],
-            device_id=z_dev(target),
-            device_id_type=MESH,
-        )
-
-    def onward(i):
-        b = nearest(i)
-        target = jnp.where(b < z, z + 1, z - 1)
-        return b, target, (target >= 0) & (target <= last)
-
-    for o in range(1, n_z):
-        rt_copy(o).start()
-    if n_z > 1:
-        for h in range(PANELS):
-
-            @pl.when(has_up)
-            def _():
-                z_copy(0, h, z, z + 1).start()
-
-            @pl.when(has_down)
-            def _():
-                z_copy(n_z, h, z, z - 1).start()
-
     def await_bytes(ref, sem):
         pltpu.make_async_copy(ref, ref, sem).wait()
-
-    def tick(distance, h):
-        for i in range(1, n_z):
-            if not (i + 1) // 2 <= distance <= i:
-                continue
-            b, target, goes_on = onward(i)
-
-            @pl.when(jnp.abs(b - z) == distance)
-            def _():
-                with scope(f"zwait{i}{h}"):
-                    await_bytes(normed.at[b, h], z_recv.at[b, h])
-
-                @pl.when(goes_on)
-                def _():
-                    z_copy(i, h, b, target).start()
 
     slot_row = lax.broadcasted_iota(jnp.int32, (slots, tok), 0)
 
@@ -309,10 +239,80 @@
         shares[b, 0] = coarse
         shares[b, 1] = (scaled - coarse.astype(F32)).astype(BF16)
 
+    loaded("route", "share")
+    routing[z, :top_count, :] = route_ref[...].astype(F32)
+    routing[z, top_count:, :] = share_ref[...]
+    choose(0)
+    loaded("x", "gain")
+    with scope("norm"):
+        for part in range(tok // 32):
+            rows = slice(part * 32, part * 32 + 32)
+            values = x_ref[rows, :].astype(F32)
+            center = jnp.mean(values, axis=1, keepdims=True)
+            spread = jnp.mean(jnp.square(values - center), axis=1, keepdims=True)
+            result = ((values - center) * lax.rsqrt(spread + NORM_EPS) * gain_ref[...]).astype(BF16)
+            for h in range(PANELS):
+                normed[z, h, rows, :] = result[:, h * panel : h * panel + panel]
+    with scope("barr"):
+        pl.semaphore_wait(barrier, n_z - 1 + plane - 1 + 2)
+
+    def rt_copy(o):
+        return pltpu.make_async_remote_copy(
+            src_ref=routing.at[z],
+            dst_ref=routing.at[z],
+            send_sem=rt_send.at[o],
+            recv_sem=rt_recv.at[z],
+            device_id=z_dev(lax.rem(z + o, n_z)),
+            device_id_type=MESH,
+        )
+
+    def z_copy(i, h, b, target):
+        return pltpu.make_async_remote_copy(
+            src_ref=normed.at[b, h],
+            dst_ref=normed.at[b, h],
+            send_sem=z_send.at[i, h],
+            recv_sem=z_recv.at[b, h],
+            device_id=z_dev(target),
+            device_id_type=MESH,
+        )
+
+    def onward(i):
+        b = nearest(i)
+        target = jnp.where(b < z, z + 1, z - 1)
+        return b, target, (target >= 0) & (target <= last)
+
+    for o in range(1, n_z):
+        rt_copy(o).start()
+    if n_z > 1:
+        for h in range(PANELS):
+
+            @pl.when(has_up)
+            def _():
+                z_copy(0, h, z, z + 1).start()
+
+            @pl.when(has_down)
+            def _():
+                z_copy(n_z, h, z, z - 1).start()
+
+    def tick(distance, h):
+        for i in range(1, n_z):
+            if not (i + 1) // 2 <= distance <= i:
+                continue
+            b, target, goes_on = onward(i)
+
+            @pl.when(jnp.abs(b - z) == distance)
+            def _():
+                with scope(f"zwait{i}{h}"):
+                    await_bytes(normed.at[b, h], z_recv.at[b, h])
+
+                @pl.when(goes_on)
+                def _():
+                    z_copy(i, h, b, target).start()
+
     def dispatch(i, h):
         b = nearest(i)
         with scope(f"disp{i}{h}"):
-            if h == 0:
+            if h == 0 and i > 0:
                 choose(i)
 
             def tile(j, _):
@@ -450,24 +450,32 @@
             place(halo[2], halo[3], WINDOW + rows_here, WINDOW)
             lax.fori_loop(0, 2, lambda i, _: attend(i * (blocks - 1), _), 0)
 
-    def send_heads():
+    def send_heads(edges):
+        each = chunk // bq
+
         def one(p, _):
             to = lax.rem(t + p, n_tp)
-            pltpu.make_async_remote_copy(
-                src_ref=att.at[pl.ds(pl.multiple_of(to * chunk, chunk), chunk)],
-                dst_ref=att_in.at[t],
-                send_sem=att_send,
-                recv_sem=att_recv,
-                device_id=(z, x, to),
-                device_id_type=MESH,
-            ).start()
+            for i in range(each):
+                block = to * each + i
+                at_edge = (block == 0) | (block == blocks - 1)
+
+                @pl.when(at_edge if edges else jnp.logical_not(at_edge))
+                def _():
+                    pltpu.make_async_remote_copy(
+                        src_ref=att.at[pl.ds(pl.multiple_of(block * bq, bq), bq)],
+                        dst_ref=att_in.at[t, i * bq : i * bq + bq],
+                        send_sem=att_send,
+                        recv_sem=att_recv,
+                        device_id=(z, x, to),
+                        device_id_type=MESH,
+                    ).start()
+
             return 0
 
         lax.fori_loop(1, n_tp, one, 0)
-        own = pl.ds(pl.multiple_of(t * chunk, chunk), chunk)
-        pltpu.make_async_copy(att.at[own], att_in.at[t], att_recv).start()
-
-    mixer_out = pltpu.make_async_copy(mixer_ref, mixer_hbm, load_sem.at[len(loads)])
+        if edges:
+            own = pl.ds(pl.multiple_of(t * chunk, chunk), chunk)
+            pltpu.make_async_copy(att.at[own], att_in.at[t], att_recv).start()
 
     def mixer():
         with scope("attwait"):
@@ -486,7 +494,6 @@
 
         with scope("mixer"):
             lax.fori_loop(0, width // TILE, tile, 0)
-        mixer_out.start()
 
     def experts(i, sent=lambda h: None):
         b = nearest(i)
@@ -554,12 +561,12 @@
         return total + jnp.dot(shares[b, 1], rows, preferred_element_type=F32)
 
     def combine(name, b, h):
-        with scope(f"retwait{name}{h}"):
+        with scope(f"retwait{name}"):
             await_bytes(returned.at[b, h], back_recv.at[b, h])
 
         @pl.when(mid)
         def _():
-            with scope(f"chain{name}{h}"):
+            with scope(f"chain{name}"):
                 await_bytes(home.at[b, h], home_recv.at[b, h])
 
         def tile(j, _):
@@ -568,18 +575,9 @@
             partial[b, h, :, cols] = total.astype(BF16)
             return 0
 
-        with scope(f"comb{name}{h}"):
+        with scope(f"comb{name}"):
             lax.fori_loop(0, panel // TILE, tile, 0)
         home_copy(b, h).start()
-
-    expert_out = [
-        pltpu.make_async_copy(
-            expert_ref.at[:, pl.ds(h * panel, panel)],
-            expert_hbm.at[:, pl.ds(h * panel, panel)],
-            load_sem.at[len(loads) + 1 + h],
-        )
-        for h in range(PANELS)
-    ]
 
     def combine_own(h):
         with scope(f"retwaitown{h}"):
@@ -605,7 +603,6 @@
 
         with scope(f"combown{h}"):
             lax.fori_loop(0, panel // TILE, tile, 0)
-        expert_out[h].start()
 
     for h in range(PANELS):
         dispatch(0, h)
@@ -623,24 +620,19 @@
         tick(2, 0)
         dispatch(2, 0)
     loaded("wg", "wu", "wd")
-    if n_z == 1:
-        send_halos()
     if n_z > 1:
         experts(0)
     if n_z > 2:
         tick(2, 1)
         dispatch(2, 1)
-    if n_z > 1:
-        send_halos()
-    if n_z > 2:
         experts(1)
         for h in range(PANELS):
             tick(3, h)
             dispatch(3, h)
+    send_halos()
+    send_heads(False)
+    if n_z > 2:
         experts(2)
-    attend_edges()
-    send_heads()
-    if n_z > 2:
 
         @pl.when(mid)
         def _():
@@ -653,19 +645,26 @@
             send_back(going_back(0), h)
 
     experts(last, sent)
+    attend_edges()
+    send_heads(True)
     for i in range(1, n_z):
         for h in range(PANELS):
             send_back(going_back(i), h)
-    mixer()
-    for i in range(last):
-        b = going_back(i)
-        if n_z > 2:
-            b = jnp.where(mid, going_back((i + 1) % last), b)
+    order = [(i, h) for i in range(last) for h in range(PANELS)]
+    if n_z > 2:
+        later = [(1, h) for h in range(PANELS)] + [(i, h) for h in range(PANELS) for i in range(2, last)]
+        at = len(later) - PANELS * (last - 2) + last - 2
         for h in range(PANELS):
-            combine(i, b, h)
-    for h in range(PANELS):
-        combine_own(h)
-
+            later.insert(at + h * (last - 1), (0, h))
+    else:
+        later = order
+    for step, ((i, h), (j, g)) in enumerate(zip(order, later)):
+        b = jnp.where(mid, going_back(j), going_back(i))
+        combine(step, b, h if g == h else jnp.where(mid, g, h))
+        if step == PANELS - 1:
+            mixer()
+    if n_z == 1:
+        mixer()
     for o in range(1, n_z):
         rt_copy(o).wait_send()
     if n_z > 1:
@@ -685,8 +684,6 @@
                 @pl.when(goes_on)
                 def _():
                     z_copy(i, h, b, target).wait_send()
-
-                home_copy(b, h).wait_send()
     for there, copies in ((has_after, to_after), (has_before, to_before)):
 
         @pl.when(there)
@@ -698,35 +695,17 @@
         for h in range(PANELS):
             gone = pl.ds(0, (plane - 1) * capacity)
             await_bytes(outgoing.at[b, h, gone], out_send.at[b, h])
+    await_bytes(att.at[pl.ds(0, (n_tp - 1) * chunk)], att_send)
+
+    for h in range(PANELS):
+        combine_own(h)
+
+    for h in range(PANELS):
+        for i in range(1, n_z):
+            home_copy(nearest(i), h).wait_send()
+        for b in range(n_z):
+            gone = pl.ds(0, (plane - 1) * capacity)
             await_bytes(produced.at[b, h, gone], back_send.at[b, h])
-    await_bytes(att.at[pl.ds(0, (n_tp - 1) * chunk)], att_send)
-    mixer_out.wait()
-    for copy in expert_out:
-        copy.wait()
-
-
-def hand_over(mixer_in, expert_in, mixer_out, expert_out, mixer_scr, expert_scr, sem):
-    steps = []
-    for source, scratch, target, at, parts in (
-        (mixer_in, mixer_scr, mixer_out, 0, 4),
-        (expert_in, expert_scr, expert_out, 4, 2),
-    ):
-        rows = source.shape[0] // parts
-        for part in range(parts):
-            here = pl.ds(part * rows, rows)
-            steps.append(
-                (
-                    pltpu.make_async_copy(source.at[here], scratch.at[here], sem.at[0, at + part]),
-                    pltpu.make_async_copy(scratch.at[here], target.at[here], sem.at[1, at + part]),
-                )
-            )
-    for take, _ in steps:
-        take.start()
-    for take, give in steps:
-        take.wait()
-        give.start()
-    for _, give in steps:
-        give.wait()
 
 
 def body(
@@ -757,6 +736,7 @@
     hidden = gate_weight.shape[2]
     tables = jnp.asarray(angle_tables(rows_here * n_ep, rows_here))
     anywhere = pl.BlockSpec(memory_space=pl.ANY)
+    vmem = pl.BlockSpec(memory_space=pltpu.VMEM)
     reach = rows_here + 2 * WINDOW
     dma = pltpu.SemaphoreType.DMA
     shapes = [
@@ -764,11 +744,11 @@
         jax.ShapeDtypeStruct((tok, width), BF16),
     ]
     both = dma((n_z, PANELS))
-    mixed, expert = pl.pallas_call(
+    return pl.pallas_call(
         functools.partial(kernel, (n_z, n_x, n_tp, top_count, capacity)),
         in_specs=[anywhere] * 13,
-        out_specs=[anywhere] * 2,
-        out_shape=shapes,
+        out_specs=[vmem] * 2,
+        out_shape=[pltpu.VMEM(s.shape, s.dtype) for s in shapes],
         scratch_shapes=[
             pltpu.SMEM(sink_logits.shape, F32),
             pltpu.VMEM((top_count, tok), jnp.int32),
@@ -780,8 +760,6 @@
             pltpu.VMEM((rows_here, kv_width), BF16),
             pltpu.VMEM((2, table_rows(rows_here), 128), F32),
             pltpu.VMEM((2, WINDOW, 128), F32),
-            pltpu.VMEM((rows_here // n_tp, width), BF16),
-            pltpu.VMEM((tok, width), BF16),
             pltpu.VMEM((kv_local, reach, HEAD_DIM), BF16),
             pltpu.VMEM((kv_local, reach, HEAD_DIM), BF16),
             pltpu.VMEM((4, WINDOW, kv_width), BF16),
@@ -816,10 +794,10 @@
             dma,
             dma((4,)),
             dma((4,)),
-            dma((15 + PANELS,)),
+            dma((14,)),
         ],
         compiler_params=pltpu.CompilerParams(
-            collective_id=0, has_side_effects=True, vmem_limit_bytes=67043328
+            collective_id=0, has_side_effects=True, vmem_limit_bytes=VMEM_BYTES
         ),
         name="layer",
     )(
@@ -837,14 +815,6 @@
         down_weight,
         mix_weight,
     )
-    return pl.pallas_call(
-        hand_over,
-        in_specs=[anywhere] * 2,
-        out_specs=[anywhere] * 2,
-        out_shape=shapes,
-        scratch_shapes=[pltpu.VMEM(s.shape, BF16) for s in shapes] + [dma((2, 6))],
-        name="hand_over",
-    )(mixed, expert)
 
 
 def z_count(mesh, n_ep):

time: 125 us -> 115 us (0.920); the launches traced: 123 us -> 115 us
  Pallas kernels: 122 us -> 112 us
  local copies, waits for them, and re-layouts: 0 us -> 1.77 us
    pallas_call x1, Pallas kernels: 120 us -> 112 us  [body(): pl.pallas_call(functools.partial(kernel, (n_z, n_x, n_tp, top_count, capa...]
    pallas_call x1 -> x0, Pallas kernels: 2.19 us -> none  [body(): pl.pallas_call(hand_over, in_specs=[anywhere] * 2, out_specs=[anywhere] *...]
    unnamed x0 -> x2, local copies, waits for them, and re-layouts: none -> 1.77 us
where the time goes in v2:
time: 115 us
  Pallas kernels  112 us (97%)
  local copies, waits for them, and re-layouts  1.77 us (2%)
    pallas_call x1, Pallas kernels, body(): pl.pallas_call(functools.partial(kernel, (n_z, n_x, n_tp, top_count, capa...  112 us

profile of v2, /device:TPU:1, one launch (start us, length us, event | category | flops | bytes accessed | tf_op | source)
XLA Modules:
  0.0 114.9 jit_solution(5046697452678800763)
XLA Ops:
  0.6 112.5 %layer.1 = (bf16[256,2048]{1,0:T(8,128)(2,1)S(1)}, bf16[128,2048]{1,0:T(8,128)(2,1)S(1)}) custom-call(f32[8]{0:T(128)} %sink_hbm.1, s32[4,128]{1,0:T(4,128)} %bitcast.4, f32[4,128]{1,0:T(4,128)} %bitcast.5, bf16[128,2048]{1,0:T(8,128)(2,1)} %x_hbm.1, f32[1,2048]{1,0:T(1,128)} %bitcast.3, bf16[1024,512]{1,0:T(8,128)(2,1)} %q_hbm.1, bf16[1024,256]{1,0:T(8,128)(2,1)} %k_hbm.1, ...), custom_call_target="tpu_custom_call" | custom-call | tf_op jit(solution)/shard_map/layer/pallas_call | solution.py:747
  113.1 1.0 copy.17
  114.1 0.8 copy.18

commit v3 on v2

--- a/solution.py
+++ b/solution.py
@@ -22,6 +22,7 @@
 MESH = pl.DeviceIdType.MESH
 PANELS = 2
 TILE = 256
+RELAYED = 256
 VMEM_BYTES = 61 << 20
 
 scope = jax.named_scope
@@ -97,6 +98,11 @@
     shares,
     partial,
     home,
+    relayed,
+    relay_shares,
+    relay_sum,
+    relay_home,
+    crossed,
     wg,
     wu,
     wd,
@@ -112,22 +118,33 @@
     back_recv,
     home_send,
     home_recv,
+    relay_send,
+    relay_recv,
+    sum_send,
+    sum_recv,
+    cross_send,
+    cross_recv,
     att_send,
     att_recv,
     halo_send,
     halo_recv,
     load_sem,
 ):
-    n_z, n_x, n_tp, top_count, capacity = sizes
+    n_z, n_x, n_y, n_tp, top_count, capacity = sizes
     n_ep = n_z * n_x
     plane = n_x * n_tp
     slots = plane * capacity
+    cores = n_tp // n_y
+    side = n_x * cores
     z, x, t = lax.axis_index("zz"), lax.axis_index("xx"), lax.axis_index("tp")
     me = x * n_tp + t
+    y, core = lax.div(t, cores), lax.rem(t, cores)
     ep = z * n_x + x
     rows_here, width_q = q_ref.shape
     tok, width = x_ref.shape
     panel = width // PANELS
+    back_width = [panel] * (PANELS - 1) + [panel - RELAYED]
+    relay_cols = pl.ds(panel - RELAYED, RELAYED)
     length = rows_here * n_ep
     kv_local = k_scr.shape[0]
     bq = WINDOW
@@ -205,7 +222,14 @@
         )
         return 0
 
+    def column(o):
+        b, row = lax.rem(z + o // n_y, n_z), lax.rem(y + o % n_y, n_y)
+        return (b, x, row * cores + core)
+
     lax.fori_loop(1, n_z, greet_z, 0)
+    for o in range(n_y + 1, n_z * n_y):
+        if o % n_y:
+            pl.semaphore_signal(barrier, inc=1, device_id=column(o), device_id_type=MESH)
     lax.fori_loop(1, plane, greet_plane, 0)
     for e in (after, before):
         pl.semaphore_signal(barrier, inc=1, device_id=ep_dev(e), device_id_type=MESH)
@@ -213,35 +237,52 @@
     def await_bytes(ref, sem):
         pltpu.make_async_copy(ref, ref, sem).wait()
 
-    slot_row = lax.broadcasted_iota(jnp.int32, (slots, tok), 0)
-
-    def choose(i):
-        b = nearest(i)
-        if i > 0:
-            await_bytes(routing.at[b], rt_recv.at[b])
-        lane_expert = (z * plane + lax.div(slot_row, capacity)).astype(F32)
+    upper = (
+        lax.broadcasted_iota(jnp.int32, (tok, tok), 0) < lax.broadcasted_iota(jnp.int32, (tok, tok), 1)
+    ).astype(F32).astype(BF16)
+
+    def pick_rows(route, expert_of_slot, count):
+        slot_row = lax.broadcasted_iota(jnp.int32, (count, tok), 0)
+        lane_expert = expert_of_slot(lax.div(slot_row, capacity)).astype(F32)
         place_in = lax.rem(slot_row, capacity).astype(F32)
-        upper = (
-            lax.broadcasted_iota(jnp.int32, (tok, tok), 0) < lax.broadcasted_iota(jnp.int32, (tok, tok), 1)
-        ).astype(F32).astype(BF16)
-        route = routing[b]
-        member = jnp.zeros((slots, tok), F32)
-        share = jnp.zeros((slots, tok), F32)
+        member = jnp.zeros((count, tok), F32)
+        share = jnp.zeros((count, tok), F32)
         for k in range(top_count):
             hit = route[k : k + 1, :] == lane_expert
             member = jnp.where(hit, 1.0, member)
             share = jnp.where(hit, route[top_count + k : top_count + k + 1, :], share)
         rank = jnp.dot(member.astype(BF16), upper, preferred_element_type=F32)
         pick = jnp.where(rank == place_in, member, 0.0)
-        picks[...] = pick.astype(BF16)
         scaled = (share * pick).T
         coarse = scaled.astype(BF16)
+        return pick, coarse, (scaled - coarse.astype(F32)).astype(BF16)
+
+    def choose(i):
+        b = nearest(i)
+        if i > 0:
+            await_bytes(routing.at[b, y], rt_recv.at[b, y])
+        pick, coarse, fine = pick_rows(routing[b, y], lambda e: z * plane + e, slots)
+        picks[...] = pick.astype(BF16)
         shares[b, 0] = coarse
-        shares[b, 1] = (scaled - coarse.astype(F32)).astype(BF16)
+        shares[b, 1] = fine
+
+    def choose_relayed(i):
+        b = nearest(i)
+
+        def expert(e):
+            return z * plane + lax.div(e, cores) * n_tp + y * cores + lax.rem(e, cores)
+
+        for o in range(n_y):
+            row = lax.rem(y + o, n_y)
+            if o > 0:
+                await_bytes(routing.at[b, row], rt_recv.at[b, row])
+            _, coarse, fine = pick_rows(routing[b, row], expert, side * capacity)
+            relay_shares[b, row, 0] = coarse
+            relay_shares[b, row, 1] = fine
 
     loaded("route", "share")
-    routing[z, :top_count, :] = route_ref[...].astype(F32)
-    routing[z, top_count:, :] = share_ref[...]
+    routing[z, y, :top_count, :] = route_ref[...].astype(F32)
+    routing[z, y, top_count:, :] = share_ref[...]
     choose(0)
     loaded("x", "gain")
     with scope("norm"):
@@ -254,15 +295,15 @@
             for h in range(PANELS):
                 normed[z, h, rows, :] = result[:, h * panel : h * panel + panel]
     with scope("barr"):
-        pl.semaphore_wait(barrier, n_z - 1 + plane - 1 + 2)
+        pl.semaphore_wait(barrier, (n_z - 1) * n_y + plane - 1 + 2)
 
     def rt_copy(o):
         return pltpu.make_async_remote_copy(
-            src_ref=routing.at[z],
-            dst_ref=routing.at[z],
+            src_ref=routing.at[z, y],
+            dst_ref=routing.at[z, y],
             send_sem=rt_send.at[o],
-            recv_sem=rt_recv.at[z],
-            device_id=z_dev(lax.rem(z + o, n_z)),
+            recv_sem=rt_recv.at[z, y],
+            device_id=column(o),
             device_id_type=MESH,
         )
 
@@ -281,7 +322,7 @@
         target = jnp.where(b < z, z + 1, z - 1)
         return b, target, (target >= 0) & (target <= last)
 
-    for o in range(1, n_z):
+    for o in range(1, n_z * n_y):
         rt_copy(o).start()
     if n_z > 1:
         for h in range(PANELS):
@@ -323,16 +364,17 @@
                 return 0
 
             lax.fori_loop(0, panel // TILE, tile, 0)
-            exchange(outgoing, arrived, out_send, out_recv, b, h)
-
-    def exchange(source, target, send, recv, b, h):
+            exchange(outgoing, arrived, out_send, out_recv, b, h, panel)
+
+    def exchange(source, target, send, recv, b, h, count):
         mine = pl.ds(pl.multiple_of(me * capacity, capacity), capacity)
+        cols = pl.ds(0, count)
 
         def one(p, _):
             to = lax.rem(me + p, plane)
             pltpu.make_async_remote_copy(
-                src_ref=source.at[b, h, pl.ds(pl.multiple_of(to * capacity, capacity), capacity)],
-                dst_ref=target.at[b, h, mine],
+                src_ref=source.at[b, h, pl.ds(pl.multiple_of(to * capacity, capacity), capacity), cols],
+                dst_ref=target.at[b, h, mine, cols],
                 send_sem=send.at[b, h],
                 recv_sem=recv.at[b, h],
                 device_id=plane_dev(to),
@@ -341,7 +383,9 @@
             return 0
 
         lax.fori_loop(1, plane, one, 0)
-        pltpu.make_async_copy(source.at[b, h, mine], target.at[b, h, mine], recv.at[b, h]).start()
+        pltpu.make_async_copy(
+            source.at[b, h, mine, cols], target.at[b, h, mine, cols], recv.at[b, h]
+        ).start()
 
     def halo_copy(source, which, start, target):
         return pltpu.make_async_remote_copy(
@@ -532,66 +576,160 @@
                 sent(h)
 
     def send_back(b, h):
-        exchange(produced, returned, back_send, back_recv, b, h)
+        exchange(produced, returned, back_send, back_recv, b, h, back_width[h])
+
+    def send_relayed(b):
+        mine = pl.ds(pl.multiple_of((x * cores + core) * capacity, capacity), capacity)
+
+        def source(to, row):
+            slot = lax.div(to, cores) * n_tp + row * cores + lax.rem(to, cores)
+            rows = pl.ds(pl.multiple_of(slot * capacity, capacity), capacity)
+            return produced.at[b, PANELS - 1, rows, relay_cols]
+
+        def one(p, _):
+            to = lax.rem(x * cores + core + p, side)
+            for row in range(n_y):
+                pltpu.make_async_remote_copy(
+                    src_ref=source(to, row),
+                    dst_ref=relayed.at[b, row, mine],
+                    send_sem=relay_send.at[b],
+                    recv_sem=relay_recv.at[b],
+                    device_id=(z, lax.div(to, cores), y * cores + lax.rem(to, cores)),
+                    device_id_type=MESH,
+                ).start()
+            return 0
+
+        lax.fori_loop(1, side, one, 0)
+        for row in range(n_y):
+            pltpu.make_async_copy(
+                source(x * cores + core, row), relayed.at[b, row, mine], relay_recv.at[b]
+            ).start()
+
+    def homeward(b):
+        target = jnp.where(b < z, z - 1, z + 1)
+        return target, jnp.where((target == b) & (b < z), n_z, b)
 
     def home_copy(b, h):
-        target = jnp.where(b < z, z - 1, z + 1)
-        slot = jnp.where((target == b) & (b < z), n_z, b)
+        target, slot = homeward(b)
+        cols = pl.ds(0, back_width[h])
         return pltpu.make_async_remote_copy(
-            src_ref=partial.at[b, h],
-            dst_ref=home.at[slot, h],
+            src_ref=partial.at[b, h, :, cols],
+            dst_ref=home.at[slot, h, :, cols],
             send_sem=home_send.at[b, h],
             recv_sem=home_recv.at[slot, h],
             device_id=z_dev(target),
             device_id_type=MESH,
         )
 
+    def relay_copy(b):
+        target, slot = homeward(b)
+        return pltpu.make_async_remote_copy(
+            src_ref=relay_sum.at[b],
+            dst_ref=relay_home.at[slot],
+            send_sem=sum_send.at[b],
+            recv_sem=sum_recv.at[slot],
+            device_id=z_dev(target),
+            device_id_type=MESH,
+        )
+
+    def cross_copy(o):
+        row = lax.rem(y + o, n_y)
+        return pltpu.make_async_remote_copy(
+            src_ref=relay_sum.at[z, row],
+            dst_ref=crossed.at[y],
+            send_sem=cross_send.at[o],
+            recv_sem=cross_recv.at[y],
+            device_id=(z, x, row * cores + core),
+            device_id_type=MESH,
+        )
+
     def clear_home():
-        for slot in range(n_z + 1):
-            from_up = (slot < z) | (slot == n_z)
-            missing = jnp.where(from_up, z == last, z == 0)
+        for slot, missing in ((z, z == 0), (n_z, z == last)):
 
             @pl.when(missing)
             def _():
                 home[slot] = jnp.zeros(home.shape[1:], BF16)
+                relay_home[slot] = jnp.zeros(relay_home.shape[1:], BF16)
 
     def weighted(b, h, cols):
         rows = returned[b, h, :, cols]
         total = jnp.dot(shares[b, 0], rows, preferred_element_type=F32)
         return total + jnp.dot(shares[b, 1], rows, preferred_element_type=F32)
 
-    def combine(name, b, h):
+    def relay_weighted(b, row):
+        rows = relayed[b, row]
+        total = jnp.dot(relay_shares[b, row, 0], rows, preferred_element_type=F32)
+        return total + jnp.dot(relay_shares[b, row, 1], rows, preferred_element_type=F32)
+
+    def combine_relayed(name, b, further):
+        with scope(f"relwait{name}"):
+            await_bytes(relayed.at[b], relay_recv.at[b])
+            if further:
+                await_bytes(relay_home.at[b], sum_recv.at[b])
+
+        with scope(f"rel{name}"):
+            for row in range(n_y):
+                total = relay_weighted(b, row)
+                if further:
+                    total = total + relay_home[b, row].astype(F32)
+                relay_sum[b, row] = total.astype(BF16)
+        relay_copy(b).start()
+
+    def from_both_sides(place, sem):
+        @pl.when(has_down)
+        def _():
+            await_bytes(place(z), sem(z))
+
+        @pl.when(has_up)
+        def _():
+            await_bytes(place(n_z), sem(n_z))
+
+    def combine_own_relayed():
+        with scope("relwaitown"):
+            await_bytes(relayed.at[z], relay_recv.at[z])
+            from_both_sides(lambda slot: relay_home.at[slot], lambda slot: sum_recv.at[slot])
+        for row in range(n_y):
+            total = relay_weighted(z, row) + relay_home[z, row].astype(F32)
+            relay_sum[z, row] = (total + relay_home[n_z, row].astype(F32)).astype(BF16)
+        for o in range(1, n_y):
+            cross_copy(o).start()
+
+    def finish_relayed():
+        total = relay_sum[z, y].astype(F32)
+        for o in range(1, n_y):
+            row = lax.rem(y + o, n_y)
+            with scope("crosswait"):
+                await_bytes(crossed.at[row], cross_recv.at[row])
+            total = total + crossed[row].astype(F32)
+        expert_ref[:, width - RELAYED :] = total.astype(BF16)
+
+    def combine(name, b, h, further):
+        cols = pl.ds(0, back_width[h])
         with scope(f"retwait{name}"):
-            await_bytes(returned.at[b, h], back_recv.at[b, h])
-
-        @pl.when(mid)
-        def _():
+            await_bytes(returned.at[b, h, :, cols], back_recv.at[b, h])
+
+        if further:
             with scope(f"chain{name}"):
-                await_bytes(home.at[b, h], home_recv.at[b, h])
+                await_bytes(home.at[b, h, :, cols], home_recv.at[b, h])
 
         def tile(j, _):
             cols = pl.ds(pl.multiple_of(j * TILE, TILE), TILE)
-            total = weighted(b, h, cols) + home[b, h, :, cols].astype(F32)
+            total = weighted(b, h, cols)
+            if further:
+                total = total + home[b, h, :, cols].astype(F32)
             partial[b, h, :, cols] = total.astype(BF16)
             return 0
 
         with scope(f"comb{name}"):
-            lax.fori_loop(0, panel // TILE, tile, 0)
+            lax.fori_loop(0, back_width[h] // TILE, tile, 0)
         home_copy(b, h).start()
 
     def combine_own(h):
+        here = pl.ds(0, back_width[h])
         with scope(f"retwaitown{h}"):
-            await_bytes(returned.at[z, h], back_recv.at[z, h])
-
+            await_bytes(returned.at[z, h, :, here], back_recv.at[z, h])
         with scope(f"homewait{h}"):
-
-            @pl.when(has_down)
-            def _():
-                await_bytes(home.at[z, h], home_recv.at[z, h])
-
-            @pl.when(has_up)
-            def _():
-                await_bytes(home.at[n_z, h], home_recv.at[n_z, h])
+            from_both_sides(lambda slot: home.at[slot, h, :, here], lambda slot: home_recv.at[slot, h])
 
         def tile(j, _):
             cols = pl.ds(pl.multiple_of(j * TILE, TILE), TILE)
@@ -602,7 +740,7 @@
             return 0
 
         with scope(f"combown{h}"):
-            lax.fori_loop(0, panel // TILE, tile, 0)
+            lax.fori_loop(0, back_width[h] // TILE, tile, 0)
 
     for h in range(PANELS):
         dispatch(0, h)
@@ -631,8 +769,16 @@
             dispatch(3, h)
     send_halos()
     send_heads(False)
+    if n_z > 1:
+        send_relayed(z)
+    if n_z > 2:
+        send_relayed(nearest(1))
+    with scope("chooserel"):
+        for i in range(n_z):
+            choose_relayed(i)
     if n_z > 2:
         experts(2)
+        send_relayed(nearest(2))
 
         @pl.when(mid)
         def _():
@@ -640,6 +786,9 @@
                 send_back(going_back(0), h)
 
     def sent(h):
+        if h == PANELS - 1:
+            send_relayed(nearest(last))
+
         @pl.when(end)
         def _():
             send_back(going_back(0), h)
@@ -650,22 +799,43 @@
     for i in range(1, n_z):
         for h in range(PANELS):
             send_back(going_back(i), h)
-    order = [(i, h) for i in range(last) for h in range(PANELS)]
+    firsts, then = [(i, None) for i in (*range(1, last), 0)][: max(last, 0)], []
+    if n_z > 1:
+        firsts += [(0, h) for h in range(PANELS)]
+        then = [(i, h) for i in range(1, last) for h in range(PANELS)]
+
+    def sums(steps, further):
+        for i, h in steps:
+            if h is None:
+                combine_relayed(i, going_back(i), further)
+            else:
+                combine(f"{i}{h}", going_back(i), h, further)
+
     if n_z > 2:
-        later = [(1, h) for h in range(PANELS)] + [(i, h) for h in range(PANELS) for i in range(2, last)]
-        at = len(later) - PANELS * (last - 2) + last - 2
-        for h in range(PANELS):
-            later.insert(at + h * (last - 1), (0, h))
+
+        @pl.when(mid)
+        def _():
+            sums([(0, None), (1, None)], True)
+
+        @pl.when(end)
+        def _():
+            sums(firsts, False)
+
+        mixer()
+
+        @pl.when(mid)
+        def _():
+            later = [(i, h) for h in range(PANELS) for i in (2, 0)]
+            sums([(2, None)] + [(1, h) for h in range(PANELS)] + later, True)
+
+        @pl.when(end)
+        def _():
+            sums(then, False)
     else:
-        later = order
-    for step, ((i, h), (j, g)) in enumerate(zip(order, later)):
-        b = jnp.where(mid, going_back(j), going_back(i))
-        combine(step, b, h if g == h else jnp.where(mid, g, h))
-        if step == PANELS - 1:
-            mixer()
-    if n_z == 1:
+        sums(firsts, False)
         mixer()
-    for o in range(1, n_z):
+    combine_own_relayed()
+    for o in range(1, n_z * n_y):
         rt_copy(o).wait_send()
     if n_z > 1:
         for h in range(PANELS):
@@ -695,20 +865,41 @@
         for h in range(PANELS):
             gone = pl.ds(0, (plane - 1) * capacity)
             await_bytes(outgoing.at[b, h, gone], out_send.at[b, h])
+        gone = pl.ds(0, (side - 1) * n_y * capacity)
+        await_bytes(produced.at[b, 0, gone, pl.ds(0, RELAYED)], relay_send.at[b])
     await_bytes(att.at[pl.ds(0, (n_tp - 1) * chunk)], att_send)
 
     for h in range(PANELS):
         combine_own(h)
-
-    for h in range(PANELS):
+        if h == 0:
+            finish_relayed()
+
+    with scope("late"):
+        for h in range(PANELS):
+            for i in range(1, n_z):
+                home_copy(nearest(i), h).wait_send()
+            for b in range(n_z):
+                gone = pl.ds(0, (plane - 1) * capacity)
+                await_bytes(produced.at[b, h, gone, pl.ds(0, back_width[h])], back_send.at[b, h])
         for i in range(1, n_z):
-            home_copy(nearest(i), h).wait_send()
-        for b in range(n_z):
-            gone = pl.ds(0, (plane - 1) * capacity)
-            await_bytes(produced.at[b, h, gone], back_send.at[b, h])
+            relay_copy(nearest(i)).wait_send()
+        for o in range(1, n_y):
+            cross_copy(o).wait_send()
+
+
+def hand_over(mixer_in, expert_in, mixer_out, expert_out, sem):
+    copies = [
+        pltpu.make_async_copy(source, target, sem.at[i])
+        for i, (source, target) in enumerate(((mixer_in, mixer_out), (expert_in, expert_out)))
+    ]
+    for copy in copies:
+        copy.start()
+    for copy in copies:
+        copy.wait()
 
 
 def body(
+    n_y,
     queries,
     key_heads,
     value_heads,
@@ -744,8 +935,9 @@
         jax.ShapeDtypeStruct((tok, width), BF16),
     ]
     both = dma((n_z, PANELS))
-    return pl.pallas_call(
-        functools.partial(kernel, (n_z, n_x, n_tp, top_count, capacity)),
+    side_slots = slots // n_y
+    mixed, expert = pl.pallas_call(
+        functools.partial(kernel, (n_z, n_x, n_y, n_tp, top_count, capacity)),
         in_specs=[anywhere] * 13,
         out_specs=[vmem] * 2,
         out_shape=[pltpu.VMEM(s.shape, s.dtype) for s in shapes],
@@ -765,7 +957,7 @@
             pltpu.VMEM((4, WINDOW, kv_width), BF16),
             pltpu.VMEM((rows_here, width_q), BF16),
             pltpu.VMEM((n_tp, rows_here // n_tp, width_q), BF16),
-            pltpu.VMEM((n_z, 2 * top_count, tok), F32),
+            pltpu.VMEM((n_z, n_y, 2 * top_count, tok), F32),
             pltpu.VMEM((n_z, PANELS, tok, panel), BF16),
             pltpu.VMEM((slots, tok), BF16),
             pltpu.VMEM((n_z, PANELS, slots, panel), BF16),
@@ -775,6 +967,11 @@
             pltpu.VMEM((n_z, 2, tok, slots), BF16),
             pltpu.VMEM((n_z, PANELS, tok, panel), BF16),
             pltpu.VMEM((n_z + 1, PANELS, tok, panel), BF16),
+            pltpu.VMEM((n_z, n_y, side_slots, RELAYED), BF16),
+            pltpu.VMEM((n_z, n_y, 2, tok, side_slots), BF16),
+            pltpu.VMEM((n_z, n_y, tok, RELAYED), BF16),
+            pltpu.VMEM((n_z + 1, n_y, tok, RELAYED), BF16),
+            pltpu.VMEM((n_y, tok, RELAYED), BF16),
             pltpu.VMEM((width, hidden), BF16),
             pltpu.VMEM((width, hidden), BF16),
             pltpu.VMEM((hidden, width), BF16),
@@ -782,14 +979,20 @@
             pltpu.VMEM((slots, hidden), BF16),
             dma((n_z + 1, PANELS)),
             both,
-            dma((n_z,)),
-            dma((n_z,)),
+            dma((n_z * n_y,)),
+            dma((n_z, n_y)),
             both,
             both,
             both,
             both,
             both,
             dma((n_z + 1, PANELS)),
+            dma((n_z,)),
+            dma((n_z,)),
+            dma((n_z,)),
+            dma((n_z + 1,)),
+            dma((n_y,)),
+            dma((n_y,)),
             dma,
             dma,
             dma((4,)),
@@ -815,21 +1018,33 @@
         down_weight,
         mix_weight,
     )
-
-
-def z_count(mesh, n_ep):
-    coords = {getattr(d, "coords", (0, 0, 0))[2] for d in mesh.devices.flat}
-    return len(coords) if len(coords) in (2, 4) and n_ep % len(coords) == 0 else 1
+    return pl.pallas_call(
+        hand_over,
+        in_specs=[vmem] * 2,
+        out_specs=[anywhere] * 2,
+        out_shape=shapes,
+        scratch_shapes=[dma((2,))],
+        name="hand_over",
+    )(
+        pltpu.with_memory_space_constraint(mixed, pltpu.VMEM),
+        pltpu.with_memory_space_constraint(expert, pltpu.VMEM),
+    )
+
+
+def count_of(mesh, axis, among):
+    coords = {getattr(d, "coords", (0, 0, 0))[axis] for d in mesh.devices.flat}
+    return len(coords) if among % len(coords) == 0 else 1
 
 
 def solution(mesh):
     n_ep, n_tp = mesh.shape["ep"], mesh.shape["tp"]
-    n_z = z_count(mesh, n_ep)
+    n_z, n_y = count_of(mesh, 2, n_ep), count_of(mesh, 1, n_tp)
+    n_z = n_z if n_z in (1, 2, 4) else 1
     grid = Mesh(mesh.devices.reshape(n_z, n_ep // n_z, n_tp), ("zz", "xx", "tp"))
     ep = ("zz", "xx")
     every = ("zz", "xx", "tp")
     return jax.shard_map(
-        body,
+        functools.partial(body, n_y),
         mesh=grid,
         in_specs=(
             P(ep, "tp"),

time: 115 us -> 110 us (0.957)
  Pallas kernels: 112 us -> 108 us
  local copies, waits for them, and re-layouts: 1.77 us -> 0 us
    pallas_call x1 -> x2, Pallas kernels: 112 us -> 108 us  [the longest x1 107 us: body(): pl.pallas_call(functools.partial(kernel, (n_z, n_x, n_y, n_tp, top_count,...]
    unnamed x2 -> x0, local copies, waits for them, and re-layouts: 1.77 us -> none
where the time goes in v3:
time: 110 us; the launch traced here: 109 us
  Pallas kernels  108 us (98%)
    pallas_call x1, Pallas kernels, body(): pl.pallas_call(functools.partial(kernel, (n_z, n_x, n_y, n_tp, top_count,...  107 us

profile of v3, /device:TPU:1, one launch (start us, length us, event | category | flops | bytes accessed | tf_op | source)
XLA Modules:
  0.0 109.1 jit_solution(2905374531831148604)
XLA Ops:
  0.6 107.2 %layer.1 = (bf16[256,2048]{1,0:T(8,128)(2,1)S(1)}, bf16[128,2048]{1,0:T(8,128)(2,1)S(1)}) custom-call(f32[8]{0:T(128)} %sink_hbm.1, s32[4,128]{1,0:T(4,128)} %bitcast.4, f32[4,128]{1,0:T(4,128)} %bitcast.5, bf16[128,2048]{1,0:T(8,128)(2,1)} %x_hbm.1, f32[1,2048]{1,0:T(1,128)} %bitcast.3, bf16[1024,512]{1,0:T(8,128)(2,1)} %q_hbm.1, bf16[1024,256]{1,0:T(8,128)(2,1)} %k_hbm.1, ...), custom_call_target="tpu_custom_call" | custom-call | tf_op jit(solution)/shard_map/layer/pallas_call | solution.py:939
  107.8 1.2 %hand_over.1 = (bf16[256,2048]{1,0:T(8,128)(2,1)}, bf16[128,2048]{1,0:T(8,128)(2,1)}) custom-call(bf16[256,2048]{1,0:T(8,128)(2,1)S(1)} %get-tuple-element.4.mixer_in, bf16[128,2048]{1,0:T(8,128)(2,1)S(1)} %get-tuple-element.5.expert_in), custom_call_target="tpu_custom_call" | custom-call | tf_op jit(solution)/shard_map/hand_over/pallas_call | solution.py:1021

commit v4 on v3

--- a/solution.py
+++ b/solution.py
@@ -363,12 +363,15 @@
                 ).astype(BF16)
                 return 0
 
-            lax.fori_loop(0, panel // TILE, tile, 0)
-            exchange(outgoing, arrived, out_send, out_recv, b, h, panel)
-
-    def exchange(source, target, send, recv, b, h, count):
+            parts = 2 if i == 0 and h == 0 else 1
+            each = panel // parts
+            for part in range(parts):
+                lax.fori_loop(part * each // TILE, (part + 1) * each // TILE, tile, 0)
+                exchange(outgoing, arrived, out_send, out_recv, b, h, each, part * each)
+
+    def exchange(source, target, send, recv, b, h, count, at=0):
         mine = pl.ds(pl.multiple_of(me * capacity, capacity), capacity)
-        cols = pl.ds(0, count)
+        cols = pl.ds(at, count)
 
         def one(p, _):
             to = lax.rem(me + p, plane)
@@ -793,48 +796,58 @@
         def _():
             send_back(going_back(0), h)
 
-    experts(last, sent)
-    attend_edges()
-    send_heads(True)
-    for i in range(1, n_z):
-        for h in range(PANELS):
-            send_back(going_back(i), h)
-    firsts, then = [(i, None) for i in (*range(1, last), 0)][: max(last, 0)], []
-    if n_z > 1:
-        firsts += [(0, h) for h in range(PANELS)]
-        then = [(i, h) for i in range(1, last) for h in range(PANELS)]
-
-    def sums(steps, further):
+    def sums(steps, further=False):
         for i, h in steps:
             if h is None:
                 combine_relayed(i, going_back(i), further)
             else:
                 combine(f"{i}{h}", going_back(i), h, further)
 
+    def all_of(i):
+        return [(i, h) for h in range(PANELS)]
+
+    experts(last, sent)
     if n_z > 2:
+
+        @pl.when(end)
+        def _():
+            sums([(2, None), (1, None)])
+
+    attend_edges()
+    send_heads(True)
+    for i in range(1, n_z):
+        for h in range(PANELS if i < last else PANELS - 1):
+            send_back(going_back(i), h)
+    if n_z > 2:
+
+        @pl.when(end)
+        def _():
+            sums([(0, None)] + all_of(0))
+            mixer()
+            sums(all_of(1))
 
         @pl.when(mid)
         def _():
             sums([(0, None), (1, None)], True)
+            mixer()
+            sums([(2, None)] + all_of(1), True)
+    else:
+        if n_z > 1:
+            sums([(0, None)] + all_of(0))
+        mixer()
+    combine_own_relayed()
+    if n_z > 1:
+        send_back(z, PANELS - 1)
+    if n_z > 2:
 
         @pl.when(end)
         def _():
-            sums(firsts, False)
-
-        mixer()
+            sums(all_of(2))
 
         @pl.when(mid)
         def _():
-            later = [(i, h) for h in range(PANELS) for i in (2, 0)]
-            sums([(2, None)] + [(1, h) for h in range(PANELS)] + later, True)
-
-        @pl.when(end)
-        def _():
-            sums(then, False)
-    else:
-        sums(firsts, False)
-        mixer()
-    combine_own_relayed()
+            sums([(i, h) for h in range(PANELS) for i in (2, 0)], True)
+
     for o in range(1, n_z * n_y):
         rt_copy(o).wait_send()
     if n_z > 1:

time: 110 us -> 109 us (level)
  no operation moved by 1% of the time
where the time goes in v4:
time: 109 us
  Pallas kernels  108 us (99%)
    pallas_call x1, Pallas kernels, body(): pl.pallas_call(functools.partial(kernel, (n_z, n_x, n_y, n_tp, top_count,...  107 us

profile of v4, /device:TPU:1, one launch (start us, length us, event | category | flops | bytes accessed | tf_op | source)
XLA Modules:
  0.0 108.6 jit_solution(6262899404417929865)
XLA Ops:
  0.6 106.6 %layer.1 = (bf16[256,2048]{1,0:T(8,128)(2,1)S(1)}, bf16[128,2048]{1,0:T(8,128)(2,1)S(1)}) custom-call(f32[8]{0:T(128)} %sink_hbm.1, s32[4,128]{1,0:T(4,128)} %bitcast.4, f32[4,128]{1,0:T(4,128)} %bitcast.5, bf16[128,2048]{1,0:T(8,128)(2,1)} %x_hbm.1, f32[1,2048]{1,0:T(1,128)} %bitcast.3, bf16[1024,512]{1,0:T(8,128)(2,1)} %q_hbm.1, bf16[1024,256]{1,0:T(8,128)(2,1)} %k_hbm.1, ...), custom_call_target="tpu_custom_call" | custom-call | tf_op jit(solution)/shard_map/layer/pallas_call | solution.py:952
  107.3 1.2 %hand_over.1 = (bf16[256,2048]{1,0:T(8,128)(2,1)}, bf16[128,2048]{1,0:T(8,128)(2,1)}) custom-call(bf16[256,2048]{1,0:T(8,128)(2,1)S(1)} %get-tuple-element.4.mixer_in, bf16[128,2048]{1,0:T(8,128)(2,1)S(1)} %get-tuple-element.5.expert_in), custom_call_target="tpu_custom_call" | custom-call | tf_op jit(solution)/shard_map/hand_over/pallas_call | solution.py:1034

commit v5 on v4

--- a/solution.py
+++ b/solution.py
@@ -366,7 +366,7 @@
             parts = 2 if i == 0 and h == 0 else 1
             each = panel // parts
             for part in range(parts):
-                lax.fori_loop(part * each // TILE, (part + 1) * each // TILE, tile, 0)
+                lax.fori_loop(part * each // TILE, (part + 1) * each // TILE, tile, 0, unroll=i == 0)
                 exchange(outgoing, arrived, out_send, out_recv, b, h, each, part * each)
 
     def exchange(source, target, send, recv, b, h, count, at=0):
@@ -743,7 +743,7 @@
             return 0
 
         with scope(f"combown{h}"):
-            lax.fori_loop(0, back_width[h] // TILE, tile, 0)
+            lax.fori_loop(0, back_width[h] // TILE, tile, 0, unroll=True)
 
     for h in range(PANELS):
         dispatch(0, h)

time: 109 us -> 108 us (level)
  no operation moved by 1% of the time
where the time goes in v5:
time: 108 us
  Pallas kernels  107 us (99%)
    pallas_call x1, Pallas kernels, body(): pl.pallas_call(functools.partial(kernel, (n_z, n_x, n_y, n_tp, top_count,...  106 us

profile of v5, /device:TPU:1, one launch (start us, length us, event | category | flops | bytes accessed | tf_op | source)
XLA Modules:
  0.0 108.2 jit_solution(4515476887319724204)
XLA Ops:
  0.6 106.2 %layer.1 = (bf16[256,2048]{1,0:T(8,128)(2,1)S(1)}, bf16[128,2048]{1,0:T(8,128)(2,1)S(1)}) custom-call(f32[8]{0:T(128)} %sink_hbm.1, s32[4,128]{1,0:T(4,128)} %bitcast.4, f32[4,128]{1,0:T(4,128)} %bitcast.5, bf16[128,2048]{1,0:T(8,128)(2,1)} %x_hbm.1, f32[1,2048]{1,0:T(1,128)} %bitcast.3, bf16[1024,512]{1,0:T(8,128)(2,1)} %q_hbm.1, bf16[1024,256]{1,0:T(8,128)(2,1)} %k_hbm.1, ...), custom_call_target="tpu_custom_call" | custom-call | tf_op jit(solution)/shard_map/layer/pallas_call | solution.py:952
  106.9 1.2 %hand_over.1 = (bf16[256,2048]{1,0:T(8,128)(2,1)}, bf16[128,2048]{1,0:T(8,128)(2,1)}) custom-call(bf16[256,2048]{1,0:T(8,128)(2,1)S(1)} %get-tuple-element.4.mixer_in, bf16[128,2048]{1,0:T(8,128)(2,1)S(1)} %get-tuple-element.5.expert_in), custom_call_target="tpu_custom_call" | custom-call | tf_op jit(solution)/shard_map/hand_over/pallas_call | solution.py:1034
